TPU v7x, 32 devices: a whole 2x2x4 slice. The times are simulated.
32 devices in a mesh: fs: 16 (over z, y, x), tp: 2 (over core).
Axes of the slice: x: 2, y: 2, z: 4, core: 2. Of those that a mesh axis runs over, the one named last changes fastest.
Arguments:
- saved_inputs: bfloat16 [2048, 4096], P('fs', 'tp'), may hold values from -6 to 6
- value_cotangent: bfloat16 [2048, 2048], P('fs'), may hold values from -0.1875 to 0.1875
- glu_output: bfloat16 [2048, 2048], P('fs', 'tp'), may hold values from -6 to 6
- conv_cotangent: bfloat16 [2048, 2048], P('fs', 'tp'), may hold values from -0.125 to 0.125
- factor: bfloat16 [4096, 256], P('tp'), may hold values from -0.09375 to 0.09375
- value_weight: float32 [2048, 4096], P('fs', 'tp'), may hold values from -3 to 3
- first_moment: float32 [2048, 256], P('fs', 'tp'), may hold values from -6 to 6
- second_moment: float32 [2048, 256], P('fs', 'tp'), may hold values from 0.25 to 4
- kernel: float32 [31, 2048], P(None, 'tp'), may hold values from -1 to 1
- kernel_first: float32 [31, 2048], P(None, 'tp'), may hold values from -6 to 6
- kernel_second: float32 [31, 2048], P(None, 'tp'), may hold values from 0.25 to 4
Outputs:
- new_value: float32 [2048, 4096], P('fs', 'tp')
- value_copy: bfloat16 [2048, 4096], P('fs', 'tp')
- value_step: float32 [2048, 4096], P('fs', 'tp')
- new_first: float32 [2048, 256], P('fs', 'tp')
- new_second: float32 [2048, 256], P('fs', 'tp')
- new_kernel: float32 [31, 2048], P(None, 'tp')
- new_kernel_first: float32 [31, 2048], P(None, 'tp')
- new_kernel_second: float32 [31, 2048], P(None, 'tp')
All inputs are finite; a program needn't handle non-finite values.
Results may differ from a plain program's by a relative error of at most 0.0055.
Values may be sent and summed in bfloat16 or wider, within the bound.
No kernel may reach another device: no remote copies, remote signals or barrier semaphores. Data moves between devices by JAX's collectives and lax.ppermute only.
A program may use at most 64 MiB of HBM per device.

v0:
```python
import jax
import jax.numpy as jnp
from jax import lax
from jax.sharding import PartitionSpec as P

WIDTH = 4096


def from_behind(x, axis, by):
    peers = lax.axis_size(axis)
    pairs = [(i, i + by) for i in range(peers) if 0 <= i + by < peers]
    return lax.ppermute(x, axis, pairs)


def body(
    saved_inputs,
    value_cotangent,
    glu_output,
    conv_cotangent,
    factor,
    value_weight,
    first_moment,
    second_moment,
    kernel,
    kernel_first,
    kernel_second,
):
    highest = lax.Precision.HIGHEST
    factor_f = factor.astype(jnp.float32)
    partial_reduced = jnp.dot(saved_inputs, factor, preferred_element_type=jnp.float32)
    reduced = lax.psum_scatter(
        partial_reduced.astype(jnp.bfloat16), "tp", scatter_dimension=1, tiled=True
    ).astype(jnp.float32)
    upper_part = reduced.astype(jnp.bfloat16)
    lower_part = (reduced - upper_part.astype(jnp.float32)).astype(jnp.bfloat16)
    dims = (((0,), (0,)), ((), ()))
    upper_term = lax.dot_general(
        value_cotangent, upper_part, dims, preferred_element_type=jnp.float32
    )
    lower_term = lax.dot_general(
        value_cotangent, lower_part, dims, preferred_element_type=jnp.float32
    )
    projected = lax.psum_scatter(upper_term + lower_term, "fs", scatter_dimension=0, tiled=True)
    new_first = 0.8 * first_moment + 0.2 * projected
    new_second = 0.9 * second_moment + 0.1 * projected * projected
    direction = new_first / jnp.sqrt(new_second)
    full_direction = lax.all_gather(direction, "tp", axis=1, tiled=True)
    back_proj = jnp.dot(full_direction, factor_f.T, precision=highest)
    row_squares = lax.psum(jnp.sum(back_proj * back_proj, axis=1), "tp")
    value_step = back_proj / jnp.sqrt(row_squares / WIDTH + 0.01)[:, None]
    new_value = value_weight - 0.05 * value_step
    value_copy = new_value.astype(jnp.bfloat16)
    token_count = glu_output.shape[0]
    reach = kernel.shape[0] - 1
    halo_rows = from_behind(glu_output[token_count - reach :], "fs", 1)
    extended = jnp.concatenate([halo_rows, glu_output], axis=0).astype(jnp.float32)
    cotangent_f = conv_cotangent.astype(jnp.float32)
    pieces = []
    for offset in range(kernel.shape[0]):
        begin = reach - offset
        pieces.append(jnp.sum(extended[begin : begin + token_count] * cotangent_f, axis=0))
    local_grad = jnp.stack(pieces, axis=0)
    kernel_grad = lax.psum(local_grad, "fs")
    new_kernel_first = 0.8 * kernel_first + 0.2 * kernel_grad
    new_kernel_second = 0.9 * kernel_second + 0.1 * kernel_grad * kernel_grad
    new_kernel = kernel - 0.05 * new_kernel_first / jnp.sqrt(new_kernel_second)
    return (
        new_value,
        value_copy,
        value_step,
        new_first,
        new_second,
        new_kernel,
        new_kernel_first,
        new_kernel_second,
    )


def solution(mesh):
    placed = (
        P("fs", "tp"),
        P("fs", None),
        P("fs", "tp"),
        P("fs", "tp"),
        P("tp", None),
        P("fs", "tp"),
        P("fs", "tp"),
        P("fs", "tp"),
        P(None, "tp"),
        P(None, "tp"),
        P(None, "tp"),
    )
    return jax.shard_map(
        body,
        mesh=mesh,
        in_specs=placed,
        out_specs=(
            P("fs", "tp"),
            P("fs", "tp"),
            P("fs", "tp"),
            P("fs", "tp"),
            P("fs", "tp"),
            P(None, "tp"),
            P(None, "tp"),
            P(None, "tp"),
        ),
        check_vma=False,
    )
```

profile of v0, /device:TPU:0, one launch (start us, length us, event | category | flops | bytes accessed | tf_op | source)
XLA Modules:
  0.0 225.3 jit_solution(7543839092658024599)
XLA Ops:
  8.0 0.0 copy-start
  8.0 0.0 reduce-scatter.7.cloned.1.call-start
  8.1 0.9 slice.96
  9.0 4.9 %collective-permute-start = (bf16[30,1024]{1,0:T(8,128)(2,1)S(1)}, bf16[30,1024]{1,0:T(8,128)(2,1)S(1)}, u32[]{:S(2)}, u32[]{:S(2)}) collective-permute-start(bf16[30,1024]{1,0:T(8,128)(2,1)S(1)} %slice.96), channel_id=1, source_target_pairs={{0,2},{2,4},{4,6},{6,8},{8,10},{10,12},{12,14},{14,16},{16,18},{18... | collective-permute-start | bytes 184328 | tf_op jit(solution)/shard_map/ppermute | solution.py:12
  13.9 0.0 copy-done
  13.9 0.0 copy-start.4
  13.9 1.4 convolution_convert_fusion
  15.3 0.7 copy.27
  16.0 0.0 reduce-scatter.7.cloned.1.call-update
  16.1 0.0 copy-start.3
  16.1 0.0 all-reduce.2.cloned.1.call-start
  16.1 0.0 collective-permute-done
  16.1 0.0 copy-done.4
  16.1 0.1 maximum_convert_fusion
  16.2 0.8 copy-done.3
  17.0 1.1 fusion.31
  18.1 0.8 fusion.30
  18.9 0.0 copy-start.1
  18.9 2.7 %stack.127 = f32[31,1024]{1,0:T(8,128)} concatenate(f32[1,1024]{1,0:T(1,128)S(1)} %bitcast.75, f32[1,1024]{1,0:T(1,128)S(1)} %bitcast.46, f32[1,1024]{1,0:T(1,128)S(1)} %bitcast.47, f32[1,1024]{1,0:T(1,128)S(1)} %bitcast.48, f32[1,1024]{1,0:T(1,128)S(1)} %bitcast.49, f32[1,1024]{1,0:T(1,128)S(1)} %bitcast.50, f32[1,1024]{1,0:T(1,128)S(1)} %bitcast.51, f32[1,1024]{1,0:T(1,128)S(1)} %bitcast.52, ...), dimensions={0} | concatenate | bytes 253952 | tf_op jit(solution)/shard_map/stack | solution.py:62
  21.6 0.0 all-reduce.2.cloned.1.call-update
  21.6 0.0 reduce-scatter.5.cloned.1.call-start
  21.7 2.4 %reduce-scatter.7.cloned.1.call-done = bf16[128,128]{1,0:T(8,128)(2,1)} async-done(((bf16[256,128]{1,0:T(8,128)(2,1)}), bf16[128,128]{1,0:T(8,128)(2,1)}) %reduce-scatter.7.cloned.1.call-update) | async-done | bytes 32784
  24.1 0.0 copy-start.8
  24.1 0.9 copy.28
  25.0 0.0 copy-done.1
  25.0 0.0 copy-done.8
  25.0 0.3 fusion.34
  25.3 1.3 fusion
  26.6 0.0 copy-start.9
  26.6 0.0 reduce-scatter.5.cloned.1.call-update
  26.6 0.8 copy-done.9
  27.5 0.1 copy.24
  27.6 0.0 copy-done.10
  27.6 0.1 copy.23
  27.7 100.1 %all-reduce.2.cloned.1.call-done = f32[31,1024]{1,0:T(8,128)} async-done(((f32[31,1024]{1,0:T(8,128)}), f32[31,1024]{1,0:T(8,128)}) %all-reduce.2.cloned.1.call-update) | async-done | bytes 126992 | tf_op jit(solution)/shard_map/psum | solution.py:63
  127.7 0.0 copy-done.7
  127.7 0.0 copy-done.5
  127.7 0.0 copy-done.6
  127.7 1.7 multiply_subtract_fusion.1
  129.4 78.8 %reduce-scatter.5.cloned.1.call-done = f32[128,128]{0,1:T(8,128)} async-done(((f32[2048,128]{0,1:T(8,128)}), f32[128,128]{0,1:T(8,128)}) %reduce-scatter.5.cloned.1.call-update) | async-done | bytes 65552 | tf_op jit(solution)/shard_map/reduce_scatter | solution.py:43
  208.2 0.9 rsqrt_multiply_fusion
  209.1 1.9 all_gather.3
  211.0 1.1 multiply_reduce_fusion
  212.1 2.5 %psum.14 = f32[128]{0:T(128)S(1)} all-reduce(f32[128]{0:T(128)S(1)} %get-tuple-element.64), channel_id=1, replica_groups=mesh['fs'=16,'tp'=2] {'tp'}, use_global_device_ids=true, to_apply=%region_3.0 | all-reduce | flops 128 | bytes 1024 | tf_op jit(solution)/shard_map/psum | solution.py:49
  214.5 0.7 copy.25
  215.3 0.7 copy.26
  216.0 0.0 copy-done.2
  216.0 1.8 fusion.37
  (6 shorter events, 0.0 us)
Async XLA Ops:
  8.0 5.9 %copy-start = (bf16[2048,256]{1,0:T(8,128)(2,1)S(1)}, bf16[2048,256]{1,0:T(8,128)(2,1)}, u32[]{:S(2)}) copy-start(bf16[2048,256]{1,0:T(8,128)(2,1)} %param.15) | copy-start | bytes 3145732
  8.0 16.1 %reduce-scatter.7.cloned.1.call-start = ((), (), s32[]{:S(2)}) async-start(), calls=%async_computation.4 | async-start | bytes 98304
  9.0 7.1 %collective-permute-start = (bf16[30,1024]{1,0:T(8,128)(2,1)S(1)}, bf16[30,1024]{1,0:T(8,128)(2,1)S(1)}, u32[]{:S(2)}, u32[]{:S(2)}) collective-permute-start(bf16[30,1024]{1,0:T(8,128)(2,1)S(1)} %slice.96), channel_id=1, source_target_pairs={{0,2},{2,4},{4,6},{6,8},{8,10},{10,12},{12,14},{14,16},{16,18},{18... | collective-permute-start | bytes 184328 | tf_op jit(solution)/shard_map/ppermute | solution.py:12
  13.9 2.2 copy-start.4
  16.1 1.0 copy-start.3
  16.1 111.7 %all-reduce.2.cloned.1.call-start = ((), (), s32[]{:S(2)}) async-start(), calls=%async_computation.3 | async-start | bytes 262144 | tf_op jit(solution)/shard_map/psum | solution.py:63
  18.9 6.1 %copy-start.1 = (bf16[128,2048]{1,0:T(8,128)(2,1)S(1)}, bf16[128,2048]{1,0:T(8,128)(2,1)}, u32[]{:S(2)}) copy-start(bf16[128,2048]{1,0:T(8,128)(2,1)} %param.12) | copy-start | bytes 1572868
  21.6 186.6 %reduce-scatter.5.cloned.1.call-start = ((), (), s32[]{:S(2)}) async-start(), calls=%async_computation.2 | async-start | bytes 1114112 | tf_op jit(solution)/shard_map/reduce_scatter | solution.py:43
  24.1 1.0 copy-start.8
  26.6 0.8 copy-start.9
  26.6 0.9 copy-start.10
  26.6 101.1 %copy-start.7 = (f32[31,1024]{1,0:T(8,128)S(1)}, f32[31,1024]{1,0:T(8,128)}, u32[]{:S(2)}) copy-start(f32[31,1024]{1,0:T(8,128)} %param.21) | copy-start | bytes 380932
  27.5 100.3 %copy-start.5 = (f32[31,1024]{1,0:T(8,128)S(1)}, f32[31,1024]{1,0:T(8,128)}, u32[]{:S(2)}) copy-start(f32[31,1024]{1,0:T(8,128)} %param.19) | copy-start | bytes 380932
  27.5 100.3 %copy-start.6 = (f32[31,1024]{1,0:T(8,128)S(1)}, f32[31,1024]{1,0:T(8,128)}, u32[]{:S(2)}) copy-start(f32[31,1024]{1,0:T(8,128)} %param.20) | copy-start | bytes 380932
  211.0 5.0 %copy-start.2 = (f32[128,2048]{1,0:T(8,128)S(1)}, f32[128,2048]{1,0:T(8,128)}, u32[]{:S(2)}) copy-start(f32[128,2048]{1,0:T(8,128)} %param.16) | copy-start | bytes 3145732
Sparse Core Ops, SparseCore 0:
  16.2 7.8 reduce-scatter.6
Sparse Core Ops, SparseCore 1:
  22.6 105.1 all-reduce.1
  130.4 77.7 reduce-scatter.4
where the time goes:
time: 226 us; the launch traced here: 225 us
  waiting for transfers between devices  181 us (80%)
  between operations  15.6 us (7%)
  local copies, waits for them, and re-layouts  8.54 us (4%)
  other arithmetic  6.33 us (3%)
  starting transfers between devices  5 us (2%)
  blocking collectives  4.37 us (2%)
  matrix products  4.05 us (2%)
    psum x1, waiting for transfers between devices, body(): kernel_grad = lax.psum(local_grad, 'fs')  100 us
    reduce_scatter x1, waiting for transfers between devices, body(): lax.psum_scatter(upper_term + lower_term, 'fs', scatter_dimension=0, tile...  78.8 us
    unnamed x28, local copies, waits for them, and re-layouts  4.95 us
    ppermute x1, starting transfers between devices, from_behind(): return lax.ppermute(x, axis, pairs)  4.87 us
  transfers between devices with their start and end apart: 4, of which 3 were waited for; matrix products, arithmetic and copies ran while one was open for 5% of the time, Pallas kernels for 0%

commit v1 on v0

v1 whole, which is shorter than its diff:
```python
import jax
import jax.numpy as jnp
from jax import lax
from jax.sharding import PartitionSpec as P

WIDTH = 4096


def from_behind(x, axis, by):
    peers = lax.axis_size(axis)
    pairs = [(i, i + by) for i in range(peers) if 0 <= i + by < peers]
    return lax.ppermute(x, axis, pairs)


def scatter_columns(partial, axis):
    peers = lax.axis_size(axis)
    me = lax.axis_index(axis)
    cols = partial.shape[1] // peers
    total = lax.dynamic_slice_in_dim(partial, me * cols, cols, axis=1)
    for by in range(1, peers):
        target = (me + by) % peers
        block = lax.dynamic_slice_in_dim(partial, target * cols, cols, axis=1)
        pairs = [(i, (i + by) % peers) for i in range(peers)]
        total = total + lax.ppermute(block.astype(jnp.bfloat16), axis, pairs).astype(jnp.float32)
    return total


def sum_peers(x, axis):
    peers = lax.axis_size(axis)
    total = x
    for by in range(1, peers):
        pairs = [(i, (i + by) % peers) for i in range(peers)]
        total = total + lax.ppermute(x, axis, pairs)
    return total


def body(
    saved_inputs,
    value_cotangent,
    glu_output,
    conv_cotangent,
    factor,
    value_weight,
    first_moment,
    second_moment,
    kernel,
    kernel_first,
    kernel_second,
):
    bf16 = jnp.bfloat16
    peers = lax.axis_size("fs")
    taps, channels = kernel.shape

    partial_reduced = jnp.dot(saved_inputs, factor, preferred_element_type=jnp.float32)
    reduced = scatter_columns(partial_reduced, "tp").astype(bf16)
    dims = (((0,), (0,)), ((), ()))
    grad_term = lax.dot_general(value_cotangent, reduced, dims, preferred_element_type=jnp.float32)
    rows = grad_term.shape[0] // peers
    blocks = grad_term.astype(bf16).reshape(peers, rows, grad_term.shape[1])
    received = lax.all_to_all(blocks, "fs", split_axis=0, concat_axis=0, tiled=True)
    projected = jnp.sum(received.astype(jnp.float32), axis=0)

    gram_part = lax.dot_general(factor, factor, dims, preferred_element_type=jnp.float32)
    gram = sum_peers(gram_part, "tp")

    new_first = 0.8 * first_moment + 0.2 * projected
    new_second = 0.9 * second_moment + 0.1 * projected * projected
    direction = new_first / jnp.sqrt(new_second)
    full_direction = lax.all_gather(direction.astype(bf16), "tp", axis=1, tiled=True)
    back_proj = lax.dot_general(
        full_direction, factor, (((1,), (1,)), ((), ())), preferred_element_type=jnp.float32
    )
    wide = full_direction.astype(jnp.float32)
    row_squares = jnp.sum(jnp.dot(wide, gram, precision=lax.Precision.HIGHEST) * wide, axis=1)
    value_step = back_proj * lax.rsqrt(row_squares / WIDTH + 0.01)[:, None]
    new_value = value_weight - 0.05 * value_step
    value_copy = new_value.astype(bf16)

    token_count = glu_output.shape[0]
    reach = taps - 1
    halo_rows = from_behind(glu_output[token_count - reach :], "fs", 1)
    extended = jnp.concatenate([halo_rows, glu_output], axis=0).astype(jnp.float32)
    cotangent_f = conv_cotangent.astype(jnp.float32)
    pieces = []
    for offset in range(taps):
        begin = reach - offset
        pieces.append(jnp.sum(extended[begin : begin + token_count] * cotangent_f, axis=0))
    local_grad = jnp.stack(pieces, axis=0).astype(bf16)
    share = -(-channels * taps // peers)
    share = -(-share // 128) * 128
    flat = jnp.pad(local_grad.reshape(-1), (0, share * peers - taps * channels))
    parts = lax.all_to_all(flat.reshape(peers, share), "fs", split_axis=0, concat_axis=0, tiled=True)
    summed = jnp.sum(parts.astype(jnp.float32), axis=0).astype(bf16)
    gathered = lax.all_gather(summed, "fs", axis=0, tiled=True)
    kernel_grad = gathered[: taps * channels].reshape(taps, channels).astype(jnp.float32)
    new_kernel_first = 0.8 * kernel_first + 0.2 * kernel_grad
    new_kernel_second = 0.9 * kernel_second + 0.1 * kernel_grad * kernel_grad
    new_kernel = kernel - 0.05 * new_kernel_first / jnp.sqrt(new_kernel_second)
    return (
        new_value,
        value_copy,
        value_step,
        new_first,
        new_second,
        new_kernel,
        new_kernel_first,
        new_kernel_second,
    )


def solution(mesh):
    wide = P("fs", "tp")
    taps = P(None, "tp")
    return jax.shard_map(
        body,
        mesh=mesh,
        in_specs=(wide, P("fs", None), wide, wide, P("tp", None), wide, wide, wide, taps, taps, taps),
        out_specs=(wide, wide, wide, wide, wide, taps, taps, taps),
        check_vma=False,
    )
```

time: 226 us -> 81 us (0.36)
  waiting for transfers between devices: 181 us -> 6.25 us
  blocking collectives: 4.37 us -> 43.1 us
  between operations: 15.6 us -> 1.14 us
  starting transfers between devices: 5 us -> 15.3 us
  local copies, waits for them, and re-layouts: 8.54 us -> 5.52 us
    psum x1 -> x0, waiting for transfers between devices: 100 us -> none  [body(): kernel_grad = lax.psum(local_grad, 'fs')]
    reduce_scatter x1 -> x0, waiting for transfers between devices: 78.8 us -> none  [body(): lax.psum_scatter(upper_term + lower_term, 'fs', scatter_dimension=0, tile...]
    all_gather x1 -> x2, blocking collectives: 1.9 us -> 43.1 us  [the longest x1 41.3 us: body(): gathered = lax.all_gather(summed, 'fs', axis=0, tiled=True)]
    all_to_all x0 -> x2, starting transfers between devices: none -> 9.81 us  [the longest x1 6.23 us: body(): lax.all_to_all(flat.reshape(peers, share), 'fs', split_axis=0, concat_axi...]
    all_to_all x0 -> x2, waiting for transfers between devices: none -> 6.25 us  [the longest x1 6.24 us: body(): lax.all_to_all(flat.reshape(peers, share), 'fs', split_axis=0, concat_axi...]
    unnamed x28 -> x22, local copies, waits for them, and re-layouts: 4.95 us -> 2.47 us
    psum x1 -> x0, blocking collectives: 2.47 us -> none  [body(): row_squares = lax.psum(jnp.sum(back_proj * back_proj, axis=1), 'tp')]
    unnamed x4 -> x0, waiting for transfers between devices: 2.46 us -> none
  transfers between devices with their start and end apart: 4 -> 5, of which waited for: 3 -> 1; matrix products, arithmetic and copies ran while one was open for 5% -> 12% of each run, Pallas kernels for 0% -> 0%
where the time goes in v1:
time: 81 us; the launch traced here: 80.5 us
  blocking collectives  43.1 us (53%)
  starting transfers between devices  15.3 us (19%)
  waiting for transfers between devices  6.25 us (8%)
  local copies, waits for them, and re-layouts  5.52 us (7%)
  other arithmetic  4.64 us (6%)
  matrix products  4.46 us (6%)
  between operations  1.14 us (1%)
    all_gather x1, blocking collectives, body(): gathered = lax.all_gather(summed, 'fs', axis=0, tiled=True)  41.3 us
    all_to_all x1, waiting for transfers between devices, body(): lax.all_to_all(flat.reshape(peers, share), 'fs', split_axis=0, concat_axi...  6.24 us
    all_to_all x1, starting transfers between devices, body(): lax.all_to_all(flat.reshape(peers, share), 'fs', split_axis=0, concat_axi...  6.23 us
    ppermute x1, starting transfers between devices, from_behind(): return lax.ppermute(x, axis, pairs)  4.87 us
    all_to_all x1, starting transfers between devices, body(): lax.all_to_all(blocks, 'fs', split_axis=0, concat_axis=0, tiled=True)  3.57 us
    unnamed x22, local copies, waits for them, and re-layouts  2.47 us
    dot_general x1, matrix products, body(): lax.dot_general(full_direction, factor, (((1,), (1,)), ((), ())), preferr...  1.97 us
    reduce_sum x2, other arithmetic, body(): jnp.sum(extended[begin:begin + token_count] * cotangent_f, axis=0)  1.9 us
  transfers between devices with their start and end apart: 5, of which 1 were waited for; matrix products, arithmetic and copies ran while one was open for 12% of the time, Pallas kernels for 0%

profile of v1, /device:TPU:0, one launch (start us, length us, event | category | flops | bytes accessed | tf_op | source)
XLA Modules:
  0.0 80.5 jit_solution(5672737794390836252)
XLA Ops:
  0.6 0.0 copy-start
  0.6 0.9 %slice.107 = bf16[30,1024]{1,0:T(8,128)(2,1)S(1)} slice(bf16[128,1024]{1,0:T(8,128)(2,1)} %param.13), slice={[98:128], [0:1024]} | slice | bytes 122880 | tf_op jit(solution)/shard_map/slice | solution.py:81
  1.6 4.9 %collective-permute-start.2 = (bf16[30,1024]{1,0:T(8,128)(2,1)S(1)}, bf16[30,1024]{1,0:T(8,128)(2,1)S(1)}, u32[]{:S(2)}, u32[]{:S(2)}) collective-permute-start(bf16[30,1024]{1,0:T(8,128)(2,1)S(1)} %slice.107), channel_id=1, source_target_pairs={{0,2},{2,4},{4,6},{6,8},{8,10},{10,12},{12,14},{14,16},{16,18},{18... | collective-permute-start | bytes 184328 | tf_op jit(solution)/shard_map/ppermute | solution.py:12
  6.5 0.0 copy-done
  6.5 1.4 %fusion.40 = f32[128,256]{1,0:T(8,128)S(1)} fusion(bf16[128,2048]{1,0:T(8,128)(2,1)} %param.11, bf16[2048,256]{1,0:T(8,128)(2,1)S(1)} %copy-done), kind=kOutput, calls=%fused_computation.86 | convolution fusion | flops 134217728 | bytes 1703936 | tf_op jit(solution)/shard_map/dot_general | solution.py:54
  7.9 0.0 copy-start.4
  7.9 0.1 collective-permute-start
  8.0 0.5 fusion.41
  8.5 0.6 collective-permute-start.1
  9.0 0.0 collective-permute-done.2
  9.0 0.0 copy-done.4
  9.0 0.1 maximum_convert_fusion
  9.1 0.9 %copy-done.2 = bf16[128,1024]{1,0:T(8,128)(2,1)S(1)} copy-done((bf16[128,1024]{1,0:T(8,128)(2,1)S(1)}, bf16[128,1024]{1,0:T(8,128)(2,1)}, u32[]{:S(2)}) %copy-start.2) | copy-done | bytes 262168
  10.0 1.1 %fusion.32 = (bf16[1024]{0:T(1024)(128)(2,1)S(1)}, bf16[1024]{0:T(1024)(128)(2,1)S(1)}, bf16[1024]{0:T(1024)(128)(2,1)S(1)}, bf16[1024]{0:T(1024)(128)(2,1)S(1)}...) fusion(bf16[128,1024]{1,0:T(8,128)(2,1)S(1)} %copy-done.2, ...), kind=kLoop, calls=%fused_computation.68 | loop fusion | flops 4831232 | bytes 9736192 | tf_op jit(solution)/shard_map/reduce_sum | solution.py:87
  11.0 0.8 %fusion.31 = (bf16[1024]{0:T(1024)(128)(2,1)S(1)}, bf16[1024]{0:T(1024)(128)(2,1)S(1)}, bf16[1024]{0:T(1024)(128)(2,1)S(1)}, bf16[1024]{0:T(1024)(128)(2,1)S(1)}...) fusion(bf16[128,1024]{1,0:T(8,128)(2,1)S(1)} %copy-done.2, ...), kind=kLoop, calls=%fused_computation.67 | loop fusion | flops 3525632 | bytes 7104512 | tf_op jit(solution)/shard_map/reduce_sum | solution.py:87
  12.3 0.0 copy-start.3
  12.3 0.3 stack.159
  12.6 0.1 convert_element_type.59
  12.7 0.5 broadcast.12
  13.2 1.0 %reduce.2 = bf16[16,2048]{1,0:T(8,128)(2,1)S(1)} reduce(bf16[16,1,2048]{2,1,0:T(2,128)(2,1)S(1)} %all_to_all.12, bf16[]{:T(256)} %broadcast.12), dimensions={1}, to_apply=%all_to_all.12.reduce_sub_computation | reduce | bytes 131074 | tf_op jit(solution)/shard_map/all_to_all | solution.py:92
  14.2 0.7 reshape.44
  14.9 6.2 %all-to-all-start.1 = ((bf16[16,2,1024]{2,1,0:T(2,128)(2,1)}), bf16[16,2,1024]{2,1,0:T(2,128)(2,1)S(1)}, u32[]{:S(2)}, u32[]{:S(2)}) async-start(bf16[16,2,1024]{2,1,0:T(2,128)(2,1)} %reshape.44), calls=%async_computation.1 | async-start | bytes 131072 | tf_op jit(solution)/shard_map/all_to_all | solution.py:92
  21.1 0.0 collective-permute-done
  21.1 0.0 copy-done.3
  21.1 0.3 fusion
  21.5 0.9 %copy.28 = bf16[16,16,8,128]{3,2,0,1:T(8,128)(2,1)} copy(bf16[16,16,8,128]{3,2,1,0:T(8,128)(2,1)S(1)} %fusion) | data formatting | bytes 1048576 | tf_op jit(solution)/shard_map/reshape | solution.py:59
  22.4 6.2 %all-to-all-done.1 = bf16[16,2,1024]{2,1,0:T(2,128)(2,1)S(1)} async-done(((bf16[16,2,1024]{2,1,0:T(2,128)(2,1)}), bf16[16,2,1024]{2,1,0:T(2,128)(2,1)S(1)}, u32[]{:S(2)}, u32[]{:S(2)}) %all-to-all-start.1) | async-done | bytes 65568 | tf_op jit(solution)/shard_map/all_to_all | solution.py:92
  28.6 3.6 %all-to-all-start = ((bf16[16,128,128]{1,2,0:T(8,128)(2,1)}), bf16[16,128,128]{1,2,0:T(8,128)(2,1)S(1)}, u32[]{:S(2)}, u32[]{:S(2)}) async-start(bf16[16,128,128]{1,2,0:T(8,128)(2,1)} %bitcast.13), calls=%async_computation | async-start | bytes 1048576 | tf_op jit(solution)/shard_map/all_to_all | solution.py:60
  32.2 0.1 reshape.45
  32.3 0.0 copy-start.6
  32.3 0.0 copy-start.7
  32.3 0.1 reduce_sum.342
  32.4 41.3 %all_gather.7 = bf16[32768]{0:T(1024)(128)(2,1)S(1)} all-gather(bf16[2048]{0:T(1024)(128)(2,1)S(1)} %reduce_sum.342), channel_id=1, replica_groups=mesh['fs'=16,'tp'=2] {'fs'}, dimensions={0}, use_global_device_ids=true | all-gather | bytes 69632 | tf_op jit(solution)/shard_map/all_gather | solution.py:94
  73.7 0.0 copy-start.5
  73.8 0.0 copy-done.6
  73.8 0.0 copy-done.7
  73.8 0.8 %copy-done.5 = f32[31,1024]{1,0:T(8,128)S(1)} copy-done((f32[31,1024]{1,0:T(8,128)S(1)}, f32[31,1024]{1,0:T(8,128)}, u32[]{:S(2)}) %copy-start.5) | copy-done | bytes 127000
  74.6 0.8 multiply_subtract_fusion.1
  75.4 0.0 all-to-all-done
  75.4 0.1 convert_reduce_fusion
  75.5 0.1 copy.21
  75.6 0.0 copy-done.8
  75.6 0.0 copy-done.9
  75.6 0.7 multiply_convert_fusion
  76.3 1.9 %all_gather.6 = bf16[128,256]{1,0:T(8,128)(2,1)S(1)} all-gather(bf16[128,128]{1,0:T(8,128)(2,1)S(1)} %get-tuple-element.44), channel_id=1, replica_groups=mesh['fs'=16,'tp'=2] {'tp'}, dimensions={1}, use_global_device_ids=true | all-gather | bytes 98304 | tf_op jit(solution)/shard_map/all_gather | solution.py:69
  78.1 0.0 collective-permute-done.1
  78.2 0.3 fusion.1
  78.5 2.0 %fusion.38 = (bf16[128,2048]{1,0:T(8,128)(2,1)}, f32[128,2048]{1,0:T(8,128)}, f32[128,2048]{1,0:T(8,128)}) fusion(f32[128,2048]{1,0:T(8,128)S(1)} %copy-done.1, f32[128]{0:T(128)S(1)} %add_rsqrt_fusion, bf16[128,256]{1,0:T(8,128)(2,1)S(1)} %all_gather.6, bf16[2048,256]{1,0:T(8,128)(2,1)S(1)} %copy-done), kind=kOutput, calls=%fused_computation.85 | convolution fusion | flops 135266304 | bytes 4784640 | tf_op jit(solution)/shard_map/dot_general | solution.py:70
  (42 shorter events, 0.3 us)
Async XLA Ops:
  0.6 5.9 %copy-start = (bf16[2048,256]{1,0:T(8,128)(2,1)S(1)}, bf16[2048,256]{1,0:T(8,128)(2,1)}, u32[]{:S(2)}) copy-start(bf16[2048,256]{1,0:T(8,128)(2,1)} %param.15) | copy-start | bytes 3145732
  1.6 7.4 %collective-permute-start.2 = (bf16[30,1024]{1,0:T(8,128)(2,1)S(1)}, bf16[30,1024]{1,0:T(8,128)(2,1)S(1)}, u32[]{:S(2)}, u32[]{:S(2)}) collective-permute-start(bf16[30,1024]{1,0:T(8,128)(2,1)S(1)} %slice.107), channel_id=1, source_target_pairs={{0,2},{2,4},{4,6},{6,8},{8,10},{10,12},{12,14},{14,16},{16,18},{18... | collective-permute-start | bytes 184328 | tf_op jit(solution)/shard_map/ppermute | solution.py:12
  7.9 1.1 %copy-start.4 = (bf16[128,1024]{1,0:T(8,128)(2,1)S(1)}, bf16[128,1024]{1,0:T(8,128)(2,1)}, u32[]{:S(2)}) copy-start(bf16[128,1024]{1,0:T(8,128)(2,1)} %param.13) | copy-start | bytes 786436
  7.9 13.2 %collective-permute-start = (bf16[128,128]{1,0:T(8,128)(2,1)S(1)}, bf16[128,128]{1,0:T(8,128)(2,1)S(1)}, u32[]{:S(2)}, u32[]{:S(2)}) collective-permute-start(bf16[128,128]{1,0:T(8,128)(2,1)S(1)} %dynamic-slice_convert_fusion), channel_id=1, source_target_pairs={{0,1},{1,0},{2,3},{3,2},{4,5},{5,4},{6,7},{7,6},{8,9},{9,8},{10,11... | collective-permute-start | bytes 98312 | tf_op jit(solution)/shard_map/ppermute | solution.py:24
  8.5 69.7 %collective-permute-start.1 = (f32[256,256]{1,0:T(8,128)S(1)}, f32[256,256]{1,0:T(8,128)S(1)}, u32[]{:S(2)}, u32[]{:S(2)}) collective-permute-start(f32[256,256]{1,0:T(8,128)S(1)} %fusion.41), channel_id=1, source_target_pairs={{0,1},{1,0},{2,3},{3,2},{4,5},{5,4},{6,7},{7,6},{8,9},{9,8},{10,11... | collective-permute-start | bytes 786440 | tf_op jit(solution)/shard_map/ppermute | solution.py:33
  9.0 0.9 %copy-start.2 = (bf16[128,1024]{1,0:T(8,128)(2,1)S(1)}, bf16[128,1024]{1,0:T(8,128)(2,1)}, u32[]{:S(2)}) copy-start(bf16[128,1024]{1,0:T(8,128)(2,1)} %param.14) | copy-start | bytes 786436
  12.3 8.8 %copy-start.3 = (bf16[128,2048]{1,0:T(8,128)(2,1)S(1)}, bf16[128,2048]{1,0:T(8,128)(2,1)}, u32[]{:S(2)}) copy-start(bf16[128,2048]{1,0:T(8,128)(2,1)} %param.12) | copy-start | bytes 1572868
  14.9 13.8 %all-to-all-start.1 = ((bf16[16,2,1024]{2,1,0:T(2,128)(2,1)}), bf16[16,2,1024]{2,1,0:T(2,128)(2,1)S(1)}, u32[]{:S(2)}, u32[]{:S(2)}) async-start(bf16[16,2,1024]{2,1,0:T(2,128)(2,1)} %reshape.44), calls=%async_computation.1 | async-start | bytes 131072 | tf_op jit(solution)/shard_map/all_to_all | solution.py:92
  28.6 46.8 %all-to-all-start = ((bf16[16,128,128]{1,2,0:T(8,128)(2,1)}), bf16[16,128,128]{1,2,0:T(8,128)(2,1)S(1)}, u32[]{:S(2)}, u32[]{:S(2)}) async-start(bf16[16,128,128]{1,2,0:T(8,128)(2,1)} %bitcast.13), calls=%async_computation | async-start | bytes 1048576 | tf_op jit(solution)/shard_map/all_to_all | solution.py:60
  32.3 41.5 %copy-start.6 = (f32[31,1024]{1,0:T(8,128)S(1)}, f32[31,1024]{1,0:T(8,128)}, u32[]{:S(2)}) copy-start(f32[31,1024]{1,0:T(8,128)} %param.20) | copy-start | bytes 380932
  32.3 41.5 %copy-start.7 = (f32[31,1024]{1,0:T(8,128)S(1)}, f32[31,1024]{1,0:T(8,128)}, u32[]{:S(2)}) copy-start(f32[31,1024]{1,0:T(8,128)} %param.21) | copy-start | bytes 380932
  73.7 0.9 %copy-start.5 = (f32[31,1024]{1,0:T(8,128)S(1)}, f32[31,1024]{1,0:T(8,128)}, u32[]{:S(2)}) copy-start(f32[31,1024]{1,0:T(8,128)} %param.19) | copy-start | bytes 380932
  74.6 1.0 %copy-start.8 = (f32[128,128]{1,0:T(8,128)S(1)}, f32[128,128]{1,0:T(8,128)}, u32[]{:S(2)}) copy-start(f32[128,128]{1,0:T(8,128)} %param.18) | copy-start | bytes 196612
  74.6 1.0 %copy-start.9 = (f32[128,128]{1,0:T(8,128)S(1)}, f32[128,128]{1,0:T(8,128)}, u32[]{:S(2)}) copy-start(f32[128,128]{1,0:T(8,128)} %param.17) | copy-start | bytes 196612
  75.4 3.1 %copy-start.1 = (f32[128,2048]{1,0:T(8,128)S(1)}, f32[128,2048]{1,0:T(8,128)}, u32[]{:S(2)}) copy-start(f32[128,2048]{1,0:T(8,128)} %param.16) | copy-start | bytes 3145732

commit v2 on v1

v2 whole, which is shorter than its diff:
```python
import jax
import jax.numpy as jnp
from jax import lax
from jax.experimental import pallas as pl
from jax.experimental.pallas import tpu as pltpu
from jax.sharding import PartitionSpec as P

WIDTH = 4096


def from_behind(x, axis, by):
    peers = lax.axis_size(axis)
    pairs = [(i, i + by) for i in range(peers) if 0 <= i + by < peers]
    return lax.ppermute(x, axis, pairs)


def scatter_columns(partial, axis):
    peers = lax.axis_size(axis)
    me = lax.axis_index(axis)
    cols = partial.shape[1] // peers
    total = lax.dynamic_slice_in_dim(partial, me * cols, cols, axis=1)
    for by in range(1, peers):
        target = (me + by) % peers
        block = lax.dynamic_slice_in_dim(partial, target * cols, cols, axis=1)
        pairs = [(i, (i + by) % peers) for i in range(peers)]
        total = total + lax.ppermute(block.astype(jnp.bfloat16), axis, pairs).astype(jnp.float32)
    return total


def sum_peers(x, axis):
    peers = lax.axis_size(axis)
    total = x
    for by in range(1, peers):
        pairs = [(i, (i + by) % peers) for i in range(peers)]
        total = total + lax.ppermute(x, axis, pairs)
    return total


LANES = 128
SUB = 16


def rounded(n, to):
    return -(-n // to) * to


def tap_sums(halo, tokens, cotangent, taps):
    count, channels = tokens.shape
    tiles = channels // LANES
    reach = halo.shape[0]
    depth = rounded(taps, SUB)

    def run(halo_ref, tokens_ref, cot_ref, out_ref, ext_ref, sums_ref):
        sums_ref[...] = jnp.zeros_like(sums_ref)

        def tile(l, carry):
            lanes = pl.ds(pl.multiple_of(l * LANES, LANES), LANES)
            ext_ref[pl.ds(0, reach), :] = halo_ref[:, lanes].astype(jnp.float32)
            ext_ref[pl.ds(reach, count), :] = tokens_ref[:, lanes].astype(jnp.float32)
            cot = cot_ref[:, lanes].astype(jnp.float32)
            for k in range(taps):
                window = ext_ref[pl.ds(reach - k, count), :]
                sums_ref[pl.ds(k, 1), :] = jnp.sum(window * cot, axis=0, keepdims=True)
            rows = pl.ds(pl.multiple_of(l * depth, depth), depth)
            out_ref[rows, :] = sums_ref[...].astype(out_ref.dtype)
            return carry

        lax.fori_loop(0, tiles, tile, 0)

    return pl.pallas_call(
        run,
        out_shape=jax.ShapeDtypeStruct((tiles * depth, LANES), jnp.bfloat16),
        scratch_shapes=[
            pltpu.VMEM((reach + count, LANES), jnp.float32),
            pltpu.VMEM((depth, LANES), jnp.float32),
        ],
        name="tap_sums",
    )(halo, tokens, cotangent)


def packed_blocks(reduced, cotangent, share, peers):
    cols = reduced.shape[1]
    rows = cotangent.shape[1] // peers
    dims = (((0,), (0,)), ((), ()))
    extra = share.shape[1]
    if rows % LANES or cols % SUB or extra % SUB:
        term = lax.dot_general(reduced, cotangent, dims, preferred_element_type=jnp.float32)
        term = term.astype(jnp.bfloat16).reshape(cols, peers, rows).transpose(1, 0, 2)
        return jnp.concatenate([term, share], axis=1)

    def run(reduced_ref, cot_ref, share_ref, out_ref):
        term = lax.dot_general(
            reduced_ref[...], cot_ref[...], dims, preferred_element_type=jnp.float32
        )
        for p in range(peers):
            out_ref[p, :cols, :] = term[:, p * rows : (p + 1) * rows].astype(out_ref.dtype)
            out_ref[p, cols:, :] = share_ref[p]

    return pl.pallas_call(
        run,
        out_shape=jax.ShapeDtypeStruct((peers, cols + extra, rows), jnp.bfloat16),
        name="packed_blocks",
    )(reduced, cotangent, share)


def updated_taps(grads, kernel, kernel_first, kernel_second):
    taps, channels = kernel.shape
    tiles = channels // LANES
    depth = grads.shape[0] // tiles

    def run(grads_ref, kernel_ref, first_ref, second_ref, out_ref, out_first_ref, out_second_ref):
        for l in range(tiles):
            lanes = pl.ds(l * LANES, LANES)
            grad = grads_ref[pl.ds(l * depth, depth), :].astype(jnp.float32)[:taps]
            first = 0.8 * first_ref[:, lanes] + 0.2 * grad
            second = 0.9 * second_ref[:, lanes] + 0.1 * grad * grad
            out_first_ref[:, lanes] = first
            out_second_ref[:, lanes] = second
            out_ref[:, lanes] = kernel_ref[:, lanes] - 0.05 * first * lax.rsqrt(second)

    like = jax.ShapeDtypeStruct(kernel.shape, jnp.float32)
    return pl.pallas_call(run, out_shape=(like, like, like), name="updated_taps")(
        grads, kernel, kernel_first, kernel_second
    )


def body(
    saved_inputs,
    value_cotangent,
    glu_output,
    conv_cotangent,
    factor,
    value_weight,
    first_moment,
    second_moment,
    kernel,
    kernel_first,
    kernel_second,
):
    bf16 = jnp.bfloat16
    peers = lax.axis_size("fs")
    taps = kernel.shape[0]
    token_count = glu_output.shape[0]

    reach = rounded(taps - 1, SUB)
    halo_rows = from_behind(glu_output[token_count - reach :], "fs", 1)
    local_grad = tap_sums(halo_rows, glu_output, conv_cotangent, taps)

    partial_reduced = jnp.dot(saved_inputs, factor, preferred_element_type=jnp.float32)
    reduced = scatter_columns(partial_reduced, "tp").astype(bf16)
    cols = reduced.shape[1]
    rows = value_cotangent.shape[1] // peers
    share = local_grad.reshape(peers, -1, rows)
    blocks = packed_blocks(reduced, value_cotangent, share, peers)
    received = lax.all_to_all(blocks, "fs", split_axis=0, concat_axis=0, tiled=True)
    share_sum = jnp.sum(received[:, cols:].astype(jnp.float32), axis=0).astype(bf16)
    projected = jnp.sum(received[:, :cols].astype(jnp.float32), axis=0).T

    copies = jnp.broadcast_to(share_sum[None], share.shape)
    grads = lax.all_to_all(copies, "fs", split_axis=0, concat_axis=0, tiled=True)

    dims = (((0,), (0,)), ((), ()))
    gram_part = lax.dot_general(factor, factor, dims, preferred_element_type=jnp.float32)
    gram = sum_peers(gram_part, "tp")

    new_first = 0.8 * first_moment + 0.2 * projected
    new_second = 0.9 * second_moment + 0.1 * projected * projected
    direction = new_first * lax.rsqrt(new_second)
    full_direction = lax.all_gather(direction.astype(bf16), "tp", axis=1, tiled=True)
    back_proj = lax.dot_general(
        full_direction, factor, (((1,), (1,)), ((), ())), preferred_element_type=jnp.float32
    )
    wide = full_direction.astype(jnp.float32)
    row_squares = jnp.sum(jnp.dot(wide, gram, precision=lax.Precision.HIGHEST) * wide, axis=1)
    value_step = back_proj * lax.rsqrt(row_squares / WIDTH + 0.01)[:, None]
    new_value = value_weight - 0.05 * value_step
    value_copy = new_value.astype(bf16)

    new_kernel, new_kernel_first, new_kernel_second = updated_taps(
        grads.reshape(local_grad.shape), kernel, kernel_first, kernel_second
    )
    return (
        new_value,
        value_copy,
        value_step,
        new_first,
        new_second,
        new_kernel,
        new_kernel_first,
        new_kernel_second,
    )


def solution(mesh):
    wide = P("fs", "tp")
    taps = P(None, "tp")
    return jax.shard_map(
        body,
        mesh=mesh,
        in_specs=(wide, P("fs", None), wide, wide, P("tp", None), wide, wide, wide, taps, taps, taps),
        out_specs=(wide, wide, wide, wide, wide, taps, taps, taps),
        check_vma=False,
    )
```

time: 81 us -> 56.5 us (0.70)
  blocking collectives: 43.1 us -> 1.87 us
  waiting for transfers between devices: 6.25 us -> 19.4 us
  Pallas kernels: 0 us -> 7.22 us
  other arithmetic: 4.64 us -> 1.41 us
  starting transfers between devices: 15.3 us -> 17.1 us
  local copies, waits for them, and re-layouts: 5.52 us -> 4.06 us
    all_gather x1 -> x0, blocking collectives: 41.3 us -> none  [body(): gathered = lax.all_gather(summed, 'fs', axis=0, tiled=True)]
    all_to_all x1, waiting for transfers between devices: 0.01 us -> 15.4 us  [body(): lax.all_to_all(blocks, 'fs', split_axis=0, concat_axis=0, tiled=True)]
    pallas_call x0 -> x3, Pallas kernels: none -> 7.22 us  [the longest x1 3.21 us: tap_sums(): pl.pallas_call(run, out_shape=jax.ShapeDtypeStruct((tiles * depth, LANES)...]
    all_to_all x1, starting transfers between devices: 3.57 us -> 7.86 us  [body(): lax.all_to_all(blocks, 'fs', split_axis=0, concat_axis=0, tiled=True)]
    all_to_all x1, waiting for transfers between devices: 6.24 us -> 2.63 us  [body(): lax.all_to_all(copies, 'fs', split_axis=0, concat_axis=0, tiled=True)]
    all_to_all x1, starting transfers between devices: 6.23 us -> 4.21 us  [body(): lax.all_to_all(copies, 'fs', split_axis=0, concat_axis=0, tiled=True)]
    reduce_sum x4 -> x2, other arithmetic: 2.11 us -> 0.1 us  [the longest x1 0.08 us: body(): projected = jnp.sum(received[:, :cols].astype(jnp.float32), axis=0).T]
    ppermute x1, waiting for transfers between devices: 0.01 us -> 1.34 us  [from_behind(): return lax.ppermute(x, axis, pairs)]
  transfers between devices with their start and end apart: 5 -> 5, of which waited for: 1 -> 3; matrix products, arithmetic and copies ran while one was open for 12% -> 10% of each run, Pallas kernels for 0% -> 0%
where the time goes in v2:
time: 56.5 us; the launch traced here: 56 us
  waiting for transfers between devices  19.4 us (34%)
  starting transfers between devices  17.1 us (30%)
  Pallas kernels  7.22 us (13%)
  matrix products  4.13 us (7%)
  local copies, waits for them, and re-layouts  4.06 us (7%)
  blocking collectives  1.87 us (3%)
  other arithmetic  1.41 us (2%)
  between operations  0.8 us (1%)
    all_to_all x1, waiting for transfers between devices, body(): lax.all_to_all(blocks, 'fs', split_axis=0, concat_axis=0, tiled=True)  15.4 us
    all_to_all x1, starting transfers between devices, body(): lax.all_to_all(blocks, 'fs', split_axis=0, concat_axis=0, tiled=True)  7.86 us
    ppermute x1, starting transfers between devices, from_behind(): return lax.ppermute(x, axis, pairs)  4.38 us
    all_to_all x1, starting transfers between devices, body(): lax.all_to_all(copies, 'fs', split_axis=0, concat_axis=0, tiled=True)  4.21 us
    pallas_call x1, Pallas kernels, tap_sums(): pl.pallas_call(run, out_shape=jax.ShapeDtypeStruct((tiles * depth, LANES)...  3.21 us
    all_to_all x1, waiting for transfers between devices, body(): lax.all_to_all(copies, 'fs', split_axis=0, concat_axis=0, tiled=True)  2.63 us
    unnamed x12, local copies, waits for them, and re-layouts  2.47 us
    pallas_call x1, Pallas kernels, packed_blocks(): pl.pallas_call(run, out_shape=jax.ShapeDtypeStruct((peers, cols + extra,...  2.18 us
  transfers between devices with their start and end apart: 5, of which 3 were waited for; matrix products, arithmetic and copies ran while one was open for 10% of the time, Pallas kernels for 0%

profile of v2, /device:TPU:0, one launch (start us, length us, event | category | flops | bytes accessed | tf_op | source)
XLA Modules:
  0.0 56.0 jit_solution(11810159801381193541)
XLA Ops:
  0.6 0.0 copy-start
  0.7 1.2 %copy-done = bf16[2048,256]{1,0:T(8,128)(2,1)S(1)} copy-done((bf16[2048,256]{1,0:T(8,128)(2,1)S(1)}, bf16[2048,256]{1,0:T(8,128)(2,1)}, u32[]{:S(2)}) %copy-start) | copy-done | bytes 1048600
  1.9 1.3 %fusion.7 = f32[128,256]{1,0:T(8,128)S(1)} fusion(bf16[128,2048]{1,0:T(8,128)(2,1)} %param.11, bf16[2048,256]{1,0:T(8,128)(2,1)S(1)} %copy-done), kind=kOutput, calls=%fused_computation.16 | convolution fusion | flops 134217728 | bytes 1703936 | tf_op jit(solution)/shard_map/dot_general | solution.py:149
  3.2 0.6 collective-permute-start
  3.8 0.8 %slice.9 = bf16[32,1024]{1,0:T(8,128)(2,1)S(1)} slice(bf16[128,1024]{1,0:T(8,128)(2,1)} %tokens_ref.1), slice={[96:128], [0:1024]} | slice | bytes 131072 | tf_op jit(solution)/shard_map/slice | solution.py:146
  4.6 4.4 %collective-permute-start.1 = (bf16[32,1024]{1,0:T(8,128)(2,1)S(1)}, bf16[32,1024]{1,0:T(8,128)(2,1)S(1)}, u32[]{:S(2)}, u32[]{:S(2)}) collective-permute-start(bf16[32,1024]{1,0:T(8,128)(2,1)S(1)} %slice.9), channel_id=1, source_target_pairs={{0,2},{2,4},{4,6},{6,8},{8,10},{10,12},{12,14},{14,16},{16,18},{18... | collective-permute-start | bytes 196616 | tf_op jit(solution)/shard_map/ppermute | solution.py:14
  9.0 0.0 collective-permute-done
  9.1 0.6 %add_convert_fusion.reduced_ref = bf16[128,128]{1,0:T(8,128)(2,1)} fusion(bf16[128,128]{1,0:T(8,128)(2,1)S(1)} %collective-permute-done, f32[128,256]{1,0:T(8,128)S(1)} %fusion.7, s32[]{:T(128)S(6)} %select_n.13), kind=kLoop, calls=%fused_computation.12 | loop fusion | flops 49152 | bytes 131076 | tf_op jit(solution)/shard_map/convert_element_type | solution.py:150
  9.7 1.3 %collective-permute-done.1.halo_ref = bf16[32,1024]{1,0:T(8,128)(2,1)S(1)} collective-permute-done((bf16[32,1024]{1,0:T(8,128)(2,1)S(1)}, bf16[32,1024]{1,0:T(8,128)(2,1)S(1)}, u32[]{:S(2)}, u32[]{:S(2)}) %collective-permute-start.1) | collective-permute-done | bytes 65568 | tf_op jit(solution)/shard_map/ppermute | solution.py:14
  11.0 0.0 copy-start.3
  11.0 0.6 %copy-done.3 = bf16[32,1024]{1,0:T(8,128)(2,1)} copy-done((bf16[32,1024]{1,0:T(8,128)(2,1)}, bf16[32,1024]{1,0:T(8,128)(2,1)S(1)}, u32[]{:S(2)}) %copy-start.3) | copy-done | bytes 65560
  11.7 3.2 %tap_sums.1 = bf16[256,128]{1,0:T(8,128)(2,1)} custom-call(bf16[32,1024]{1,0:T(8,128)(2,1)} %copy-done.3, bf16[128,1024]{1,0:T(8,128)(2,1)} %tokens_ref.1, bf16[128,1024]{1,0:T(8,128)(2,1)} %cot_ref.2), custom_call_target="tpu_custom_call" | custom-call | tf_op jit(solution)/shard_map/tap_sums/pallas_call | solution.py:70
  14.9 2.2 %packed_blocks.1 = bf16[16,144,128]{2,1,0:T(8,128)(2,1)} custom-call(bf16[128,128]{1,0:T(8,128)(2,1)} %add_convert_fusion.reduced_ref, bf16[128,2048]{1,0:T(8,128)(2,1)} %cot_ref.3, bf16[16,16,128]{2,1,0:T(8,128)(2,1)} %bitcast.16), custom_call_target="tpu_custom_call" | custom-call | tf_op jit(solution)/shard_map/packed_blocks/pallas_call | solution.py:99
  17.0 7.9 %all-to-all-start = ((bf16[16,144,128]{2,1,0:T(8,128)(2,1)}), bf16[16,144,128]{2,1,0:T(8,128)(2,1)S(1)}, u32[]{:S(2)}, u32[]{:S(2)}) async-start(bf16[16,144,128]{2,1,0:T(8,128)(2,1)} %packed_blocks.1), calls=%async_computation | async-start | bytes 1179648 | tf_op jit(solution)/shard_map/all_to_all | solution.py:155
  24.9 0.0 copy-start.4
  24.9 0.0 copy-start.5
  24.9 0.5 fusion.8
  25.4 0.0 copy-start.1
  25.4 0.1 collective-permute-start.2
  25.5 15.4 %all-to-all-done = bf16[16,144,128]{2,1,0:T(8,128)(2,1)S(1)} async-done(((bf16[16,144,128]{2,1,0:T(8,128)(2,1)}), bf16[16,144,128]{2,1,0:T(8,128)(2,1)S(1)}, u32[]{:S(2)}, u32[]{:S(2)}) %all-to-all-start) | async-done | bytes 589856 | tf_op jit(solution)/shard_map/all_to_all | solution.py:155
  40.9 0.1 convert_reduce_fusion
  41.0 0.1 copy.19
  41.1 0.6 %broadcast_in_dim.2 = bf16[16,16,128]{2,1,0:T(8,128)(2,1)} broadcast(bf16[16,128]{1,0:T(8,128)(2,1)S(1)} %slice_reduce_fusion), dimensions={1,2} | broadcast | bytes 69632 | tf_op jit(solution)/shard_map/broadcast_in_dim | solution.py:159
  41.8 4.2 %all-to-all-start.1 = ((bf16[16,16,128]{2,1,0:T(8,128)(2,1)}), bf16[16,16,128]{2,1,0:T(8,128)(2,1)S(1)}, u32[]{:S(2)}, u32[]{:S(2)}) async-start(bf16[16,16,128]{2,1,0:T(8,128)(2,1)} %broadcast_in_dim.2), calls=%async_computation.1 | async-start | bytes 131072 | tf_op jit(solution)/shard_map/all_to_all | solution.py:160
  46.0 0.0 copy-done.4
  46.0 0.0 copy-done.5
  46.0 0.7 %multiply_convert_fusion = (bf16[128,128]{1,0:T(8,128)(2,1)S(1)}, f32[128,128]{1,0:T(8,128)}, f32[128,128]{1,0:T(8,128)}) fusion(f32[128,128]{0,1:T(8,128)S(1)} %copy.19, f32[128,128]{1,0:T(8,128)S(1)} %copy-done.4, f32[128,128]{1,0:T(8,128)S(1)} %copy-done.5), kind=kLoop, calls=%fused_computation.11 | loop fusion | flops 147456 | bytes 360448 | tf_op jit(solution)/shard_map/convert_element_type | solution.py:169
  46.7 1.9 %all_gather.3 = bf16[128,256]{1,0:T(8,128)(2,1)S(1)} all-gather(bf16[128,128]{1,0:T(8,128)(2,1)S(1)} %get-tuple-element.16), channel_id=1, replica_groups=mesh['fs'=16,'tp'=2] {'tp'}, dimensions={1}, use_global_device_ids=true | all-gather | bytes 98304 | tf_op jit(solution)/shard_map/all_gather | solution.py:169
  48.6 0.0 collective-permute-done.2
  48.6 0.3 fusion
  48.9 0.0 copy-done.1
  48.9 2.0 %fusion.4 = (bf16[128,2048]{1,0:T(8,128)(2,1)}, f32[128,2048]{1,0:T(8,128)}, f32[128,2048]{1,0:T(8,128)}) fusion(f32[128,2048]{1,0:T(8,128)S(1)} %copy-done.1, f32[128]{0:T(128)S(1)} %add_rsqrt_fusion, bf16[128,256]{1,0:T(8,128)(2,1)S(1)} %all_gather.3, bf16[2048,256]{1,0:T(8,128)(2,1)S(1)} %copy-done), kind=kOutput, calls=%fused_computation.15 | convolution fusion | flops 135266304 | bytes 4784640 | tf_op jit(solution)/shard_map/dot_general | solution.py:170
  50.9 2.6 %all-to-all-done.1 = bf16[16,16,128]{2,1,0:T(8,128)(2,1)S(1)} async-done(((bf16[16,16,128]{2,1,0:T(8,128)(2,1)}), bf16[16,16,128]{2,1,0:T(8,128)(2,1)S(1)}, u32[]{:S(2)}, u32[]{:S(2)}) %all-to-all-start.1) | async-done | bytes 65568 | tf_op jit(solution)/shard_map/all_to_all | solution.py:160
  53.5 0.0 copy-start.2
  53.5 0.6 %copy-done.2 = bf16[16,16,128]{2,1,0:T(8,128)(2,1)} copy-done((bf16[16,16,128]{2,1,0:T(8,128)(2,1)}, bf16[16,16,128]{2,1,0:T(8,128)(2,1)S(1)}, u32[]{:S(2)}) %copy-start.2) | copy-done | bytes 65560
  54.1 1.8 %updated_taps.1 = (f32[31,1024]{1,0:T(8,128)}, f32[31,1024]{1,0:T(8,128)}, f32[31,1024]{1,0:T(8,128)}) custom-call(bf16[256,128]{1,0:T(8,128)(2,1)} %bitcast.17, f32[31,1024]{1,0:T(8,128)} %kernel_ref.1, f32[31,1024]{1,0:T(8,128)} %first_ref.1, f32[31,1024]{1,0:T(8,128)} %second_ref.1), custom_call_target="tpu_custom_call" | custom-call | tf_op jit(solution)/shard_map/updated_taps/pallas_call | solution.py:122
  (3 shorter events, 0.0 us)
Async XLA Ops:
  0.6 1.2 %copy-start = (bf16[2048,256]{1,0:T(8,128)(2,1)S(1)}, bf16[2048,256]{1,0:T(8,128)(2,1)}, u32[]{:S(2)}) copy-start(bf16[2048,256]{1,0:T(8,128)(2,1)} %param.15) | copy-start | bytes 3145732
  3.2 5.8 %collective-permute-start = (bf16[128,128]{1,0:T(8,128)(2,1)S(1)}, bf16[128,128]{1,0:T(8,128)(2,1)S(1)}, u32[]{:S(2)}, u32[]{:S(2)}) collective-permute-start(bf16[128,128]{1,0:T(8,128)(2,1)S(1)} %dynamic-slice_convert_fusion), channel_id=1, source_target_pairs={{0,1},{1,0},{2,3},{3,2},{4,5},{5,4},{6,7},{7,6},{8,9},{9,8},{10,11... | collective-permute-start | bytes 98312 | tf_op jit(solution)/shard_map/ppermute | solution.py:26
  4.6 6.4 %collective-permute-start.1 = (bf16[32,1024]{1,0:T(8,128)(2,1)S(1)}, bf16[32,1024]{1,0:T(8,128)(2,1)S(1)}, u32[]{:S(2)}, u32[]{:S(2)}) collective-permute-start(bf16[32,1024]{1,0:T(8,128)(2,1)S(1)} %slice.9), channel_id=1, source_target_pairs={{0,2},{2,4},{4,6},{6,8},{8,10},{10,12},{12,14},{14,16},{16,18},{18... | collective-permute-start | bytes 196616 | tf_op jit(solution)/shard_map/ppermute | solution.py:14
  11.0 0.6 %copy-start.3 = (bf16[32,1024]{1,0:T(8,128)(2,1)}, bf16[32,1024]{1,0:T(8,128)(2,1)S(1)}, u32[]{:S(2)}) copy-start(bf16[32,1024]{1,0:T(8,128)(2,1)S(1)} %collective-permute-done.1.halo_ref) | copy-start | bytes 196612
  17.0 23.9 %all-to-all-start = ((bf16[16,144,128]{2,1,0:T(8,128)(2,1)}), bf16[16,144,128]{2,1,0:T(8,128)(2,1)S(1)}, u32[]{:S(2)}, u32[]{:S(2)}) async-start(bf16[16,144,128]{2,1,0:T(8,128)(2,1)} %packed_blocks.1), calls=%async_computation | async-start | bytes 1179648 | tf_op jit(solution)/shard_map/all_to_all | solution.py:155
  24.9 21.1 %copy-start.4 = (f32[128,128]{1,0:T(8,128)S(1)}, f32[128,128]{1,0:T(8,128)}, u32[]{:S(2)}) copy-start(f32[128,128]{1,0:T(8,128)} %param.18) | copy-start | bytes 196612
  24.9 21.1 %copy-start.5 = (f32[128,128]{1,0:T(8,128)S(1)}, f32[128,128]{1,0:T(8,128)}, u32[]{:S(2)}) copy-start(f32[128,128]{1,0:T(8,128)} %param.17) | copy-start | bytes 196612
  25.4 23.5 %copy-start.1 = (f32[128,2048]{1,0:T(8,128)S(1)}, f32[128,2048]{1,0:T(8,128)}, u32[]{:S(2)}) copy-start(f32[128,2048]{1,0:T(8,128)} %param.16) | copy-start | bytes 3145732
  25.4 23.1 %collective-permute-start.2 = (f32[256,256]{1,0:T(8,128)S(1)}, f32[256,256]{1,0:T(8,128)S(1)}, u32[]{:S(2)}, u32[]{:S(2)}) collective-permute-start(f32[256,256]{1,0:T(8,128)S(1)} %fusion.8), channel_id=1, source_target_pairs={{0,1},{1,0},{2,3},{3,2},{4,5},{5,4},{6,7},{7,6},{8,9},{9,8},{10,11... | collective-permute-start | bytes 786440 | tf_op jit(solution)/shard_map/ppermute | solution.py:35
  41.8 11.8 %all-to-all-start.1 = ((bf16[16,16,128]{2,1,0:T(8,128)(2,1)}), bf16[16,16,128]{2,1,0:T(8,128)(2,1)S(1)}, u32[]{:S(2)}, u32[]{:S(2)}) async-start(bf16[16,16,128]{2,1,0:T(8,128)(2,1)} %broadcast_in_dim.2), calls=%async_computation.1 | async-start | bytes 131072 | tf_op jit(solution)/shard_map/all_to_all | solution.py:160
  53.5 0.6 %copy-start.2 = (bf16[16,16,128]{2,1,0:T(8,128)(2,1)}, bf16[16,16,128]{2,1,0:T(8,128)(2,1)S(1)}, u32[]{:S(2)}) copy-start(bf16[16,16,128]{2,1,0:T(8,128)(2,1)S(1)} %all-to-all-done.1) | copy-start | bytes 196612

commit v3 on v2

--- a/solution.py
+++ b/solution.py
@@ -4,6 +4,7 @@
 from jax.experimental import pallas as pl
 from jax.experimental.pallas import tpu as pltpu
 from jax.sharding import PartitionSpec as P
+
 
 WIDTH = 4096
 
@@ -44,6 +45,16 @@
     return -(-n // to) * to
 
 
+def exchange(x, groups):
+    return lax.all_to_all(
+        x, "fs", split_axis=0, concat_axis=0, tiled=True, axis_index_groups=groups
+    )
+
+
+def on_chip(*arrays):
+    return tuple(pltpu.with_memory_space_constraint(x, pltpu.VMEM) for x in arrays)
+
+
 def tap_sums(halo, tokens, cotangent, taps):
     count, channels = tokens.shape
     tiles = channels // LANES
@@ -69,38 +80,44 @@
 
     return pl.pallas_call(
         run,
-        out_shape=jax.ShapeDtypeStruct((tiles * depth, LANES), jnp.bfloat16),
+        out_shape=pltpu.VMEM((tiles * depth, LANES), jnp.bfloat16),
         scratch_shapes=[
             pltpu.VMEM((reach + count, LANES), jnp.float32),
             pltpu.VMEM((depth, LANES), jnp.float32),
         ],
         name="tap_sums",
-    )(halo, tokens, cotangent)
-
-
-def packed_blocks(reduced, cotangent, share, peers):
+    )(*on_chip(halo, tokens, cotangent))
+
+
+def packed_blocks(reduced, cotangent, share, peers, near):
     cols = reduced.shape[1]
     rows = cotangent.shape[1] // peers
+    far = peers // near
     dims = (((0,), (0,)), ((), ()))
     extra = share.shape[1]
     if rows % LANES or cols % SUB or extra % SUB:
         term = lax.dot_general(reduced, cotangent, dims, preferred_element_type=jnp.float32)
-        term = term.astype(jnp.bfloat16).reshape(cols, peers, rows).transpose(1, 0, 2)
+        term = term.astype(jnp.bfloat16).reshape(cols, far, near, rows)
+        term = term.transpose(2, 1, 0, 3).reshape(near, far * cols, rows)
         return jnp.concatenate([term, share], axis=1)
 
     def run(reduced_ref, cot_ref, share_ref, out_ref):
         term = lax.dot_general(
             reduced_ref[...], cot_ref[...], dims, preferred_element_type=jnp.float32
         )
-        for p in range(peers):
-            out_ref[p, :cols, :] = term[:, p * rows : (p + 1) * rows].astype(out_ref.dtype)
-            out_ref[p, cols:, :] = share_ref[p]
+        for f in range(far):
+            for n in range(near):
+                p = f * near + n
+                block = term[:, p * rows : (p + 1) * rows].astype(out_ref.dtype)
+                out_ref[n, f * cols : (f + 1) * cols, :] = block
+        for n in range(near):
+            out_ref[n, far * cols :, :] = share_ref[n]
 
     return pl.pallas_call(
         run,
-        out_shape=jax.ShapeDtypeStruct((peers, cols + extra, rows), jnp.bfloat16),
+        out_shape=jax.ShapeDtypeStruct((near, far * cols + extra, rows), jnp.bfloat16),
         name="packed_blocks",
-    )(reduced, cotangent, share)
+    )(*on_chip(reduced, cotangent, share))
 
 
 def updated_taps(grads, kernel, kernel_first, kernel_second):
@@ -120,7 +137,7 @@
 
     like = jax.ShapeDtypeStruct(kernel.shape, jnp.float32)
     return pl.pallas_call(run, out_shape=(like, like, like), name="updated_taps")(
-        grads, kernel, kernel_first, kernel_second
+        *on_chip(grads, kernel, kernel_first, kernel_second)
     )
 
 
@@ -150,14 +167,22 @@
     reduced = scatter_columns(partial_reduced, "tp").astype(bf16)
     cols = reduced.shape[1]
     rows = value_cotangent.shape[1] // peers
-    share = local_grad.reshape(peers, -1, rows)
-    blocks = packed_blocks(reduced, value_cotangent, share, peers)
-    received = lax.all_to_all(blocks, "fs", split_axis=0, concat_axis=0, tiled=True)
-    share_sum = jnp.sum(received[:, cols:].astype(jnp.float32), axis=0).astype(bf16)
-    projected = jnp.sum(received[:, :cols].astype(jnp.float32), axis=0).T
-
-    copies = jnp.broadcast_to(share_sum[None], share.shape)
-    grads = lax.all_to_all(copies, "fs", split_axis=0, concat_axis=0, tiled=True)
+    near = 4 if peers % 4 == 0 else 1
+    far = peers // near
+    groups = [[f * near + n for n in range(near)] for f in range(far)]
+    across = [[f * near + n for f in range(far)] for n in range(near)]
+    share = local_grad.reshape(near, -1, rows)
+    blocks = packed_blocks(reduced, value_cotangent, share, peers, near)
+    received = exchange(blocks, groups)
+    summed = jnp.sum(received.astype(jnp.float32), axis=0).astype(bf16)
+    main = summed[: far * cols].reshape(far, cols, rows)
+    taps_part = jnp.broadcast_to(summed[far * cols :][None], (far,) + share.shape[1:])
+    received = exchange(jnp.concatenate([main, taps_part], axis=1), across)
+    total = jnp.sum(received.astype(jnp.float32), axis=0)
+    projected = total[:cols].T
+
+    copies = jnp.broadcast_to(total[cols:].astype(bf16)[None], share.shape)
+    grads = exchange(copies, groups)
 
     dims = (((0,), (0,)), ((), ()))
     gram_part = lax.dot_general(factor, factor, dims, preferred_element_type=jnp.float32)

time: 56.5 us -> 53.5 us (0.947)
  blocking collectives: 1.87 us -> 15.6 us
  waiting for transfers between devices: 19.4 us -> 10.3 us
  Pallas kernels: 7.22 us -> 3.43 us
  local copies, waits for them, and re-layouts: 4.06 us -> 2.05 us
  starting transfers between devices: 17.1 us -> 15.1 us
    all_to_all x0 -> x1, blocking collectives: none -> 13.7 us  [exchange(): lax.all_to_all(x, 'fs', split_axis=0, concat_axis=0, tiled=True, axis_ind...]
    all_to_all x2, waiting for transfers between devices: 18.1 us -> 8.48 us  [exchange(): lax.all_to_all(x, 'fs', split_axis=0, concat_axis=0, tiled=True, axis_ind...]
    pallas_call x2, Pallas kernels: 5.39 us -> 2.65 us  [the longest x1 1.51 us: tap_sums(): pl.pallas_call(run, out_shape=pltpu.VMEM((tiles * depth, LANES), jnp.bflo...]
    all_to_all x2, starting transfers between devices: 12.1 us -> 9.96 us  [exchange(): lax.all_to_all(x, 'fs', split_axis=0, concat_axis=0, tiled=True, axis_ind...]
    unnamed x12 -> x21, local copies, waits for them, and re-layouts: 2.47 us -> 1.34 us
    pallas_call x1, Pallas kernels: 1.83 us -> 0.78 us  [updated_taps(): pl.pallas_call(run, out_shape=(like, like, like), name='updated_taps')]
    slice x1, local copies, waits for them, and re-layouts: 0.84 us -> 0.01 us  [body(): halo_rows = from_behind(glu_output[token_count - reach:], 'fs', 1)]
    concatenate x0 -> x1, other arithmetic: none -> 0.69 us  [body(): received = exchange(jnp.concatenate([main, taps_part], axis=1), across)]
  transfers between devices with their start and end apart: 5 -> 5, of which waited for: 3 -> 3; matrix products, arithmetic and copies ran while one was open for 10% -> 6% of each run, Pallas kernels for 0% -> 0%
where the time goes in v3:
time: 53.5 us; the launch traced here: 53.1 us
  blocking collectives  15.6 us (29%)
  starting transfers between devices  15.1 us (28%)
  waiting for transfers between devices  10.3 us (19%)
  matrix products  4.17 us (8%)
  Pallas kernels  3.43 us (6%)
  local copies, waits for them, and re-layouts  2.05 us (4%)
  other arithmetic  1.52 us (3%)
  between operations  0.86 us (2%)
    all_to_all x1, blocking collectives, exchange(): lax.all_to_all(x, 'fs', split_axis=0, concat_axis=0, tiled=True, axis_ind...  13.7 us
    all_to_all x2, starting transfers between devices, exchange(): lax.all_to_all(x, 'fs', split_axis=0, concat_axis=0, tiled=True, axis_ind...  9.96 us
    all_to_all x2, waiting for transfers between devices, exchange(): lax.all_to_all(x, 'fs', split_axis=0, concat_axis=0, tiled=True, axis_ind...  8.48 us
    ppermute x1, starting transfers between devices, from_behind(): return lax.ppermute(x, axis, pairs)  4.54 us
    dot_general x1, matrix products, body(): lax.dot_general(full_direction, factor, (((1,), (1,)), ((), ())), preferr...  1.97 us
    all_gather x1, blocking collectives, body(): lax.all_gather(direction.astype(bf16), 'tp', axis=1, tiled=True)  1.87 us
    ppermute x1, waiting for transfers between devices, from_behind(): return lax.ppermute(x, axis, pairs)  1.85 us
    pallas_call x1, Pallas kernels, tap_sums(): pl.pallas_call(run, out_shape=pltpu.VMEM((tiles * depth, LANES), jnp.bflo...  1.51 us
  transfers between devices with their start and end apart: 5, of which 3 were waited for; matrix products, arithmetic and copies ran while one was open for 6% of the time, Pallas kernels for 0%

profile of v3, /device:TPU:0, one launch (start us, length us, event | category | flops | bytes accessed | tf_op | source)
XLA Modules:
  0.0 53.1 jit_solution(11746644409345281207)
XLA Ops:
  0.6 0.0 copy-start
  0.7 1.2 %copy-done = bf16[2048,256]{1,0:T(8,128)(2,1)S(1)} copy-done((bf16[2048,256]{1,0:T(8,128)(2,1)S(1)}, bf16[2048,256]{1,0:T(8,128)(2,1)}, u32[]{:S(2)}) %copy-start) | copy-done | bytes 1048600
  1.9 0.0 copy-start.2
  1.9 0.0 copy-start.3
  1.9 1.4 %fusion.7 = f32[128,256]{1,0:T(8,128)S(1)} fusion(bf16[128,2048]{1,0:T(8,128)(2,1)} %param.11, bf16[2048,256]{1,0:T(8,128)(2,1)S(1)} %copy-done), kind=kOutput, calls=%fused_computation.17 | convolution fusion | flops 134217728 | bytes 1703936 | tf_op jit(solution)/shard_map/dot_general | solution.py:166
  3.3 0.0 copy-start.1
  3.3 0.6 %collective-permute-start = (bf16[128,128]{1,0:T(8,128)(2,1)S(1)}, bf16[128,128]{1,0:T(8,128)(2,1)S(1)}, u32[]{:S(2)}, u32[]{:S(2)}) collective-permute-start(bf16[128,128]{1,0:T(8,128)(2,1)S(1)} %dynamic-slice_convert_fusion), channel_id=1, source_target_pairs={{0,1},{1,0},{2,3},{3,2},{4,5},{5,4},{6,7},{7,6},{8,9},{9,8},{10,11... | collective-permute-start | bytes 98312 | tf_op jit(solution)/shard_map/ppermute | solution.py:27
  3.9 0.0 copy-done.2
  3.9 4.5 %collective-permute-start.1 = (bf16[32,1024]{1,0:T(8,128)(2,1)S(1)}, bf16[32,1024]{1,0:T(8,128)(2,1)S(1)}, u32[]{:S(2)}, u32[]{:S(2)}) collective-permute-start(bf16[32,1024]{1,0:T(8,128)(2,1)S(1)} %slice.16), channel_id=1, source_target_pairs={{0,2},{2,4},{4,6},{6,8},{8,10},{10,12},{12,14},{14,16},{16,18},{18... | collective-permute-start | bytes 196616 | tf_op jit(solution)/shard_map/ppermute | solution.py:15
  8.4 0.0 collective-permute-done
  8.5 1.8 %collective-permute-done.1.halo_ref = bf16[32,1024]{1,0:T(8,128)(2,1)S(1)} collective-permute-done((bf16[32,1024]{1,0:T(8,128)(2,1)S(1)}, bf16[32,1024]{1,0:T(8,128)(2,1)S(1)}, u32[]{:S(2)}, u32[]{:S(2)}) %collective-permute-start.1) | collective-permute-done | bytes 65568 | tf_op jit(solution)/shard_map/ppermute | solution.py:15
  10.3 0.0 copy-done.3
  10.3 1.5 %tap_sums.1 = bf16[256,128]{1,0:T(8,128)(2,1)S(1)} custom-call(bf16[32,1024]{1,0:T(8,128)(2,1)S(1)} %collective-permute-done.1.halo_ref, bf16[128,1024]{1,0:T(8,128)(2,1)S(1)} %copy-done.2, bf16[128,1024]{1,0:T(8,128)(2,1)S(1)} %copy-done.3), custom_call_target="tpu_custom_call" | custom-call | tf_op jit(solution)/shard_map/tap_sums/pallas_call | solution.py:81
  11.8 0.0 copy-done.1
  11.9 1.1 %packed_blocks.1 = bf16[4,576,128]{2,1,0:T(8,128)(2,1)} custom-call(bf16[128,128]{1,0:T(8,128)(2,1)S(1)} %add_convert_fusion.reduced_ref, bf16[128,2048]{1,0:T(8,128)(2,1)S(1)} %copy-done.1, bf16[4,64,128]{2,1,0:T(8,128)(2,1)S(1)} %bitcast.17), custom_call_target="tpu_custom_call" | custom-call | tf_op jit(solution)/shard_map/packed_blocks/pallas_call | solution.py:116
  13.0 13.7 %all_to_all.15 = bf16[4,576,128]{2,1,0:T(8,128)(2,1)S(1)} all-to-all(bf16[4,576,128]{2,1,0:T(8,128)(2,1)} %packed_blocks.1), channel_id=1, replica_groups={{0,2,4,6},{8,10,12,14},{16,18,20,22},{24,26,28,30},{1,3,5,7},{9,11,13,1..., dimensions={0} | all-to-all | bytes 1179648 | tf_op jit(solution)/shard_map/all_to_all | solution.py:49
  26.7 0.1 reduce_sum.30
  26.9 0.7 %pad_maximum_fusion = bf16[4,192,128]{2,1,0:T(8,128)(2,1)} fusion(bf16[4,64,128]{2,1,0:T(8,128)(2,1)S(1)} %broadcast_in_dim.4, bf16[4,128,128]{2,1,0:T(8,128)(2,1)S(1)} %bitcast.19), kind=kLoop, calls=%fused_computation.6 | loop fusion | flops 393216 | bytes 393216 | tf_op jit(solution)/shard_map/concatenate | solution.py:180
  27.6 6.7 %all-to-all-start.1 = ((bf16[4,192,128]{2,1,0:T(8,128)(2,1)}), bf16[4,192,128]{2,1,0:T(8,128)(2,1)S(1)}, u32[]{:S(2)}, u32[]{:S(2)}) async-start(bf16[4,192,128]{2,1,0:T(8,128)(2,1)} %pad_maximum_fusion), calls=%async_computation.1 | async-start | bytes 393216 | tf_op jit(solution)/shard_map/all_to_all | solution.py:49
  34.2 0.0 copy-start.8
  34.2 0.0 copy-start.9
  34.2 0.5 fusion.8
  34.7 0.0 copy-start.7
  34.7 0.1 collective-permute-start.2
  34.8 5.7 %all-to-all-done.1 = bf16[4,192,128]{2,1,0:T(8,128)(2,1)S(1)} async-done(((bf16[4,192,128]{2,1,0:T(8,128)(2,1)}), bf16[4,192,128]{2,1,0:T(8,128)(2,1)S(1)}, u32[]{:S(2)}, u32[]{:S(2)}) %all-to-all-start.1) | async-done | bytes 196640 | tf_op jit(solution)/shard_map/all_to_all | solution.py:49
  40.5 0.1 copy.21
  40.6 0.0 copy-done.8
  40.6 0.0 copy-done.9
  40.7 0.7 %multiply_convert_fusion = (bf16[128,128]{1,0:T(8,128)(2,1)S(1)}, f32[128,128]{1,0:T(8,128)}, f32[128,128]{1,0:T(8,128)}) fusion(f32[128,128]{0,1:T(8,128)S(1)} %copy.21, f32[128,128]{1,0:T(8,128)S(1)} %copy-done.8, f32[128,128]{1,0:T(8,128)S(1)} %copy-done.9), kind=kLoop, calls=%fused_computation.11 | loop fusion | flops 147456 | bytes 360448 | tf_op jit(solution)/shard_map/convert_element_type | solution.py:194
  41.3 1.9 %all_gather.3 = bf16[128,256]{1,0:T(8,128)(2,1)S(1)} all-gather(bf16[128,128]{1,0:T(8,128)(2,1)S(1)} %get-tuple-element.16), channel_id=1, replica_groups=mesh['fs'=16,'tp'=2] {'tp'}, dimensions={1}, use_global_device_ids=true | all-gather | bytes 98304 | tf_op jit(solution)/shard_map/all_gather | solution.py:194
  43.2 0.0 collective-permute-done.2
  43.2 0.3 fusion
  43.5 0.6 %broadcast_in_dim.5 = bf16[4,64,128]{2,1,0:T(8,128)(2,1)} broadcast(bf16[64,128]{1,0:T(8,128)(2,1)S(1)} %slice.26), dimensions={1,2} | broadcast | bytes 81920 | tf_op jit(solution)/shard_map/broadcast_in_dim | solution.py:184
  44.2 3.3 %all-to-all-start.2 = ((bf16[4,64,128]{2,1,0:T(8,128)(2,1)}), bf16[4,64,128]{2,1,0:T(8,128)(2,1)S(1)}, u32[]{:S(2)}, u32[]{:S(2)}) async-start(bf16[4,64,128]{2,1,0:T(8,128)(2,1)} %broadcast_in_dim.5), calls=%async_computation.2 | async-start | bytes 131072 | tf_op jit(solution)/shard_map/all_to_all | solution.py:49
  47.5 0.0 copy-done.7
  47.5 0.0 copy-start.4
  47.5 0.0 copy-start.5
  47.5 0.0 copy-start.6
  47.5 2.0 %fusion.4 = (bf16[128,2048]{1,0:T(8,128)(2,1)}, f32[128,2048]{1,0:T(8,128)}, f32[128,2048]{1,0:T(8,128)}) fusion(f32[128,2048]{1,0:T(8,128)S(1)} %copy-done.7, f32[128]{0:T(128)S(1)} %add_rsqrt_fusion, bf16[128,256]{1,0:T(8,128)(2,1)S(1)} %all_gather.3, bf16[2048,256]{1,0:T(8,128)(2,1)S(1)} %copy-done), kind=kOutput, calls=%fused_computation.16 | convolution fusion | flops 135266304 | bytes 4784640 | tf_op jit(solution)/shard_map/dot_general | solution.py:195
  49.5 2.8 %all-to-all-done.2 = bf16[4,64,128]{2,1,0:T(8,128)(2,1)S(1)} async-done(((bf16[4,64,128]{2,1,0:T(8,128)(2,1)}), bf16[4,64,128]{2,1,0:T(8,128)(2,1)S(1)}, u32[]{:S(2)}, u32[]{:S(2)}) %all-to-all-start.2) | async-done | bytes 65568 | tf_op jit(solution)/shard_map/all_to_all | solution.py:49
  52.3 0.0 copy-done.4
  52.3 0.0 copy-done.5
  52.3 0.0 copy-done.6
  52.3 0.8 %updated_taps.1 = (f32[31,1024]{1,0:T(8,128)}, f32[31,1024]{1,0:T(8,128)}, f32[31,1024]{1,0:T(8,128)}) custom-call(bf16[256,128]{1,0:T(8,128)(2,1)S(1)} %bitcast.18, f32[31,1024]{1,0:T(8,128)S(1)} %copy-done.4, f32[31,1024]{1,0:T(8,128)S(1)} %copy-done.5, f32[31,1024]{1,0:T(8,128)S(1)} %copy-done.6), custom_call_target="tpu_custom_call" | custom-call | tf_op jit(solution)/shard_map/updated_taps/pallas_call | solution.py:139
  (10 shorter events, 0.1 us)
Async XLA Ops:
  0.6 1.2 %copy-start = (bf16[2048,256]{1,0:T(8,128)(2,1)S(1)}, bf16[2048,256]{1,0:T(8,128)(2,1)}, u32[]{:S(2)}) copy-start(bf16[2048,256]{1,0:T(8,128)(2,1)} %param.15) | copy-start | bytes 3145732
  1.9 2.0 %copy-start.2 = (bf16[128,1024]{1,0:T(8,128)(2,1)S(1)}, bf16[128,1024]{1,0:T(8,128)(2,1)}, u32[]{:S(2)}) copy-start(bf16[128,1024]{1,0:T(8,128)(2,1)} %tokens_ref.1) | copy-start | bytes 786436
  1.9 8.5 %copy-start.3 = (bf16[128,1024]{1,0:T(8,128)(2,1)S(1)}, bf16[128,1024]{1,0:T(8,128)(2,1)}, u32[]{:S(2)}) copy-start(bf16[128,1024]{1,0:T(8,128)(2,1)} %cot_ref.2) | copy-start | bytes 786436
  3.3 8.6 %copy-start.1 = (bf16[128,2048]{1,0:T(8,128)(2,1)S(1)}, bf16[128,2048]{1,0:T(8,128)(2,1)}, u32[]{:S(2)}) copy-start(bf16[128,2048]{1,0:T(8,128)(2,1)} %cot_ref.3) | copy-start | bytes 1572868
  3.3 5.1 %collective-permute-start = (bf16[128,128]{1,0:T(8,128)(2,1)S(1)}, bf16[128,128]{1,0:T(8,128)(2,1)S(1)}, u32[]{:S(2)}, u32[]{:S(2)}) collective-permute-start(bf16[128,128]{1,0:T(8,128)(2,1)S(1)} %dynamic-slice_convert_fusion), channel_id=1, source_target_pairs={{0,1},{1,0},{2,3},{3,2},{4,5},{5,4},{6,7},{7,6},{8,9},{9,8},{10,11... | collective-permute-start | bytes 98312 | tf_op jit(solution)/shard_map/ppermute | solution.py:27
  3.9 6.4 %collective-permute-start.1 = (bf16[32,1024]{1,0:T(8,128)(2,1)S(1)}, bf16[32,1024]{1,0:T(8,128)(2,1)S(1)}, u32[]{:S(2)}, u32[]{:S(2)}) collective-permute-start(bf16[32,1024]{1,0:T(8,128)(2,1)S(1)} %slice.16), channel_id=1, source_target_pairs={{0,2},{2,4},{4,6},{6,8},{8,10},{10,12},{12,14},{14,16},{16,18},{18... | collective-permute-start | bytes 196616 | tf_op jit(solution)/shard_map/ppermute | solution.py:15
  27.6 12.9 %all-to-all-start.1 = ((bf16[4,192,128]{2,1,0:T(8,128)(2,1)}), bf16[4,192,128]{2,1,0:T(8,128)(2,1)S(1)}, u32[]{:S(2)}, u32[]{:S(2)}) async-start(bf16[4,192,128]{2,1,0:T(8,128)(2,1)} %pad_maximum_fusion), calls=%async_computation.1 | async-start | bytes 393216 | tf_op jit(solution)/shard_map/all_to_all | solution.py:49
  34.2 6.4 %copy-start.8 = (f32[128,128]{1,0:T(8,128)S(1)}, f32[128,128]{1,0:T(8,128)}, u32[]{:S(2)}) copy-start(f32[128,128]{1,0:T(8,128)} %param.18) | copy-start | bytes 196612
  34.2 6.4 %copy-start.9 = (f32[128,128]{1,0:T(8,128)S(1)}, f32[128,128]{1,0:T(8,128)}, u32[]{:S(2)}) copy-start(f32[128,128]{1,0:T(8,128)} %param.17) | copy-start | bytes 196612
  34.7 12.8 %copy-start.7 = (f32[128,2048]{1,0:T(8,128)S(1)}, f32[128,2048]{1,0:T(8,128)}, u32[]{:S(2)}) copy-start(f32[128,2048]{1,0:T(8,128)} %param.16) | copy-start | bytes 3145732
  34.7 8.5 %collective-permute-start.2 = (f32[256,256]{1,0:T(8,128)S(1)}, f32[256,256]{1,0:T(8,128)S(1)}, u32[]{:S(2)}, u32[]{:S(2)}) collective-permute-start(f32[256,256]{1,0:T(8,128)S(1)} %fusion.8), channel_id=1, source_target_pairs={{0,1},{1,0},{2,3},{3,2},{4,5},{5,4},{6,7},{7,6},{8,9},{9,8},{10,11... | collective-permute-start | bytes 786440 | tf_op jit(solution)/shard_map/ppermute | solution.py:36
  44.2 8.1 %all-to-all-start.2 = ((bf16[4,64,128]{2,1,0:T(8,128)(2,1)}), bf16[4,64,128]{2,1,0:T(8,128)(2,1)S(1)}, u32[]{:S(2)}, u32[]{:S(2)}) async-start(bf16[4,64,128]{2,1,0:T(8,128)(2,1)} %broadcast_in_dim.5), calls=%async_computation.2 | async-start | bytes 131072 | tf_op jit(solution)/shard_map/all_to_all | solution.py:49
  47.5 4.8 %copy-start.4 = (f32[31,1024]{1,0:T(8,128)S(1)}, f32[31,1024]{1,0:T(8,128)}, u32[]{:S(2)}) copy-start(f32[31,1024]{1,0:T(8,128)} %kernel_ref.1) | copy-start | bytes 380932
  47.5 4.8 %copy-start.5 = (f32[31,1024]{1,0:T(8,128)S(1)}, f32[31,1024]{1,0:T(8,128)}, u32[]{:S(2)}) copy-start(f32[31,1024]{1,0:T(8,128)} %first_ref.1) | copy-start | bytes 380932
  47.5 4.8 %copy-start.6 = (f32[31,1024]{1,0:T(8,128)S(1)}, f32[31,1024]{1,0:T(8,128)}, u32[]{:S(2)}) copy-start(f32[31,1024]{1,0:T(8,128)} %second_ref.1) | copy-start | bytes 380932

commit v4 on v2

--- a/solution.py
+++ b/solution.py
@@ -4,6 +4,7 @@
 from jax.experimental import pallas as pl
 from jax.experimental.pallas import tpu as pltpu
 from jax.sharding import PartitionSpec as P
+
 
 WIDTH = 4096
 
@@ -42,6 +43,10 @@
 
 def rounded(n, to):
     return -(-n // to) * to
+
+
+def on_chip(*arrays):
+    return tuple(pltpu.with_memory_space_constraint(x, pltpu.VMEM) for x in arrays)
 
 
 def tap_sums(halo, tokens, cotangent, taps):
@@ -69,38 +74,66 @@
 
     return pl.pallas_call(
         run,
-        out_shape=jax.ShapeDtypeStruct((tiles * depth, LANES), jnp.bfloat16),
+        out_shape=pltpu.VMEM((tiles * depth, LANES), jnp.bfloat16),
         scratch_shapes=[
             pltpu.VMEM((reach + count, LANES), jnp.float32),
             pltpu.VMEM((depth, LANES), jnp.float32),
         ],
         name="tap_sums",
-    )(halo, tokens, cotangent)
-
-
-def packed_blocks(reduced, cotangent, share, peers):
+    )(*on_chip(halo, tokens, cotangent))
+
+
+def row_blocks(reduced, cotangent, peers):
     cols = reduced.shape[1]
     rows = cotangent.shape[1] // peers
     dims = (((0,), (0,)), ((), ()))
-    extra = share.shape[1]
-    if rows % LANES or cols % SUB or extra % SUB:
+    if rows % LANES or cols % SUB:
         term = lax.dot_general(reduced, cotangent, dims, preferred_element_type=jnp.float32)
-        term = term.astype(jnp.bfloat16).reshape(cols, peers, rows).transpose(1, 0, 2)
-        return jnp.concatenate([term, share], axis=1)
-
-    def run(reduced_ref, cot_ref, share_ref, out_ref):
+        return term.astype(jnp.bfloat16).reshape(cols, peers, rows).transpose(1, 0, 2)
+
+    def run(reduced_ref, cot_ref, out_ref):
         term = lax.dot_general(
             reduced_ref[...], cot_ref[...], dims, preferred_element_type=jnp.float32
         )
         for p in range(peers):
-            out_ref[p, :cols, :] = term[:, p * rows : (p + 1) * rows].astype(out_ref.dtype)
-            out_ref[p, cols:, :] = share_ref[p]
+            out_ref[p] = term[:, p * rows : (p + 1) * rows].astype(out_ref.dtype)
 
     return pl.pallas_call(
         run,
-        out_shape=jax.ShapeDtypeStruct((peers, cols + extra, rows), jnp.bfloat16),
-        name="packed_blocks",
-    )(reduced, cotangent, share)
+        out_shape=jax.ShapeDtypeStruct((peers, cols, rows), jnp.bfloat16),
+        name="row_blocks",
+    )(*on_chip(reduced, cotangent))
+
+
+def collected(x, axis, place, count, pairs_by):
+    out = lax.dynamic_update_index_in_dim(jnp.zeros((count,) + x.shape, x.dtype), x, place, 0)
+    for by in range(1, count):
+        got = lax.ppermute(x, axis, pairs_by(by))
+        out = lax.dynamic_update_index_in_dim(out, got, (place - by) % count, 0)
+    return out
+
+
+def summed_taps(local, axis):
+    peers = lax.axis_size(axis)
+    near = 4 if peers % 4 == 0 else 1
+    far = peers // near
+    me = lax.axis_index(axis)
+    n, f = me % near, me // near
+
+    def inside(by):
+        return [(g * near + i, g * near + (i + by) % near) for g in range(far) for i in range(near)]
+
+    def across(by):
+        return [(g * near + i, (g + by) % far * near + i) for g in range(far) for i in range(near)]
+
+    parts = local.reshape(near, -1, local.shape[1])
+    total = lax.dynamic_index_in_dim(parts, n, 0, keepdims=False).astype(jnp.float32)
+    for by in range(1, near):
+        block = lax.dynamic_index_in_dim(parts, (n + by) % near, 0, keepdims=False)
+        total = total + lax.ppermute(block, axis, inside(by)).astype(jnp.float32)
+    sums = collected(total.astype(local.dtype), axis, f, far, across)
+    total = jnp.sum(sums.astype(jnp.float32), axis=0).astype(local.dtype)
+    return collected(total, axis, n, near, inside).reshape(local.shape)
 
 
 def updated_taps(grads, kernel, kernel_first, kernel_second):
@@ -120,7 +153,7 @@
 
     like = jax.ShapeDtypeStruct(kernel.shape, jnp.float32)
     return pl.pallas_call(run, out_shape=(like, like, like), name="updated_taps")(
-        grads, kernel, kernel_first, kernel_second
+        *on_chip(grads, kernel, kernel_first, kernel_second)
     )
 
 
@@ -148,16 +181,9 @@
 
     partial_reduced = jnp.dot(saved_inputs, factor, preferred_element_type=jnp.float32)
     reduced = scatter_columns(partial_reduced, "tp").astype(bf16)
-    cols = reduced.shape[1]
-    rows = value_cotangent.shape[1] // peers
-    share = local_grad.reshape(peers, -1, rows)
-    blocks = packed_blocks(reduced, value_cotangent, share, peers)
+    blocks = row_blocks(reduced, value_cotangent, peers)
     received = lax.all_to_all(blocks, "fs", split_axis=0, concat_axis=0, tiled=True)
-    share_sum = jnp.sum(received[:, cols:].astype(jnp.float32), axis=0).astype(bf16)
-    projected = jnp.sum(received[:, :cols].astype(jnp.float32), axis=0).T
-
-    copies = jnp.broadcast_to(share_sum[None], share.shape)
-    grads = lax.all_to_all(copies, "fs", split_axis=0, concat_axis=0, tiled=True)
+    projected = jnp.sum(received.astype(jnp.float32), axis=0).T
 
     dims = (((0,), (0,)), ((), ()))
     gram_part = lax.dot_general(factor, factor, dims, preferred_element_type=jnp.float32)
@@ -176,8 +202,9 @@
     new_value = value_weight - 0.05 * value_step
     value_copy = new_value.astype(bf16)
 
+    grads = summed_taps(local_grad, "fs")
     new_kernel, new_kernel_first, new_kernel_second = updated_taps(
-        grads.reshape(local_grad.shape), kernel, kernel_first, kernel_second
+        grads, kernel, kernel_first, kernel_second
     )
     return (
         new_value,

time: 56.5 us -> 54.1 us (0.958)
  starting transfers between devices: 17.1 us -> 25.7 us
  waiting for transfers between devices: 19.4 us -> 13.8 us
  Pallas kernels: 7.22 us -> 3.42 us
  local copies, waits for them, and re-layouts: 4.06 us -> 1.95 us
  matrix products: 4.13 us -> 5.13 us
  other arithmetic: 1.41 us -> 0.81 us
    ppermute x0 -> x9, starting transfers between devices: none -> 15.7 us  [the longest x6 10.3 us: collected(): got = lax.ppermute(x, axis, pairs_by(by))]
    all_to_all x1, waiting for transfers between devices: 15.4 us -> 0.01 us  [body(): lax.all_to_all(blocks, 'fs', split_axis=0, concat_axis=0, tiled=True)]
    ppermute x0 -> x9, waiting for transfers between devices: none -> 13.5 us  [the longest x6 11.1 us: collected(): got = lax.ppermute(x, axis, pairs_by(by))]
    all_to_all x1 -> x0, starting transfers between devices: 4.21 us -> none  [body(): lax.all_to_all(copies, 'fs', split_axis=0, concat_axis=0, tiled=True)]
    all_to_all x1, starting transfers between devices: 7.86 us -> 5.05 us  [body(): lax.all_to_all(blocks, 'fs', split_axis=0, concat_axis=0, tiled=True)]
    pallas_call x2, Pallas kernels: 5.39 us -> 2.64 us  [the longest x1 1.51 us: tap_sums(): pl.pallas_call(run, out_shape=pltpu.VMEM((tiles * depth, LANES), jnp.bflo...]
    all_to_all x1 -> x0, waiting for transfers between devices: 2.63 us -> none  [body(): lax.all_to_all(copies, 'fs', split_axis=0, concat_axis=0, tiled=True)]
    unnamed x12 -> x20, local copies, waits for them, and re-layouts: 2.47 us -> 0.81 us
  transfers between devices with their start and end apart: 5 -> 13, of which waited for: 3 -> 7; matrix products, arithmetic and copies ran while one was open for 10% -> 5% of each run, Pallas kernels for 0% -> 6%
where the time goes in v4:
time: 54.1 us; the launch traced here: 53.8 us
  starting transfers between devices  25.7 us (48%)
  waiting for transfers between devices  13.8 us (26%)
  matrix products  5.13 us (9%)
  Pallas kernels  3.42 us (6%)
  local copies, waits for them, and re-layouts  1.95 us (4%)
  blocking collectives  1.87 us (3%)
  between operations  1.1 us (2%)
  other arithmetic  0.81 us (1%)
    ppermute x6, waiting for transfers between devices, collected(): got = lax.ppermute(x, axis, pairs_by(by))  11.1 us
    ppermute x6, starting transfers between devices, collected(): got = lax.ppermute(x, axis, pairs_by(by))  10.3 us
    ppermute x3, starting transfers between devices, summed_taps(): total = total + lax.ppermute(block, axis, inside(by)).astype(jnp.float32)  5.37 us
    all_to_all x1, starting transfers between devices, body(): lax.all_to_all(blocks, 'fs', split_axis=0, concat_axis=0, tiled=True)  5.05 us
    ppermute x1, starting transfers between devices, from_behind(): return lax.ppermute(x, axis, pairs)  4.86 us
    ppermute x3, waiting for transfers between devices, summed_taps(): total = total + lax.ppermute(block, axis, inside(by)).astype(jnp.float32)  2.43 us
    dot_general x1, matrix products, body(): lax.dot_general(full_direction, factor, (((1,), (1,)), ((), ())), preferr...  1.97 us
    all_gather x1, blocking collectives, body(): lax.all_gather(direction.astype(bf16), 'tp', axis=1, tiled=True)  1.87 us
  transfers between devices with their start and end apart: 13, of which 7 were waited for; matrix products, arithmetic and copies ran while one was open for 5% of the time, Pallas kernels for 6%

profile of v4, /device:TPU:0, one launch (start us, length us, event | category | flops | bytes accessed | tf_op | source)
XLA Modules:
  0.0 53.8 jit_solution(16476199578008157118)
XLA Ops:
  0.6 0.0 copy-start
  0.6 0.9 %slice.3 = bf16[32,1024]{1,0:T(8,128)(2,1)S(1)} slice(bf16[128,1024]{1,0:T(8,128)(2,1)} %tokens_ref.1), slice={[96:128], [0:1024]} | slice | bytes 131072 | tf_op jit(solution)/shard_map/slice | solution.py:179
  1.6 4.9 %collective-permute-start.2 = (bf16[32,1024]{1,0:T(8,128)(2,1)S(1)}, bf16[32,1024]{1,0:T(8,128)(2,1)S(1)}, u32[]{:S(2)}, u32[]{:S(2)}) collective-permute-start(bf16[32,1024]{1,0:T(8,128)(2,1)S(1)} %slice.3), channel_id=1, source_target_pairs={{0,2},{2,4},{4,6},{6,8},{8,10},{10,12},{12,14},{14,16},{16,18},{18... | collective-permute-start | bytes 196616 | tf_op jit(solution)/shard_map/ppermute | solution.py:15
  6.5 0.0 copy-start.2
  6.5 0.0 copy-start.3
  6.5 1.4 %fusion.11 = f32[128,256]{1,0:T(8,128)S(1)} fusion(bf16[128,2048]{1,0:T(8,128)(2,1)} %param.11, bf16[2048,256]{1,0:T(8,128)(2,1)S(1)} %copy-done), kind=kOutput, calls=%fused_computation.30 | convolution fusion | flops 134217728 | bytes 1703936 | tf_op jit(solution)/shard_map/dot_general | solution.py:182
  7.9 0.1 collective-permute-start
  8.1 0.2 collective-permute-done.2.halo_ref
  8.3 1.5 %tap_sums.1 = bf16[256,128]{1,0:T(8,128)(2,1)S(1)} custom-call(bf16[32,1024]{1,0:T(8,128)(2,1)S(1)} %collective-permute-done.2.halo_ref, bf16[128,1024]{1,0:T(8,128)(2,1)S(1)} %copy-done.2, bf16[128,1024]{1,0:T(8,128)(2,1)S(1)} %copy-done.3), custom_call_target="tpu_custom_call" | custom-call | tf_op jit(solution)/shard_map/tap_sums/pallas_call | solution.py:75
  9.9 3.4 %collective-permute-start.5 = (bf16[64,128]{1,0:T(8,128)(2,1)S(1)}, bf16[64,128]{1,0:T(8,128)(2,1)S(1)}, u32[]{:S(2)}, u32[]{:S(2)}) collective-permute-start(bf16[64,128]{1,0:T(8,128)(2,1)S(1)} %get-tuple-element.22), channel_id=1, source_target_pairs={{0,6},{2,0},{4,2},{6,4},{8,14},{10,8},{12,10},{14,12},{16,22},{18,... | collective-permute-start | bytes 49160 | tf_op jit(solution)/shard_map/ppermute | solution.py:133
  13.2 0.5 collective-permute-start.4
  13.8 1.5 %collective-permute-start.3 = (bf16[64,128]{1,0:T(8,128)(2,1)S(1)}, bf16[64,128]{1,0:T(8,128)(2,1)S(1)}, u32[]{:S(2)}, u32[]{:S(2)}) collective-permute-start(bf16[64,128]{1,0:T(8,128)(2,1)S(1)} %get-tuple-element.21), channel_id=1, source_target_pairs={{0,2},{2,4},{4,6},{6,0},{8,10},{10,12},{12,14},{14,8},{16,18},{18,... | collective-permute-start | bytes 49160 | tf_op jit(solution)/shard_map/ppermute | solution.py:133
  15.2 0.5 fusion.12
  15.7 0.1 collective-permute-start.1
  16.0 0.0 collective-permute-done.5
  16.0 1.0 %collective-permute-done.4 = bf16[64,128]{1,0:T(8,128)(2,1)S(1)} collective-permute-done((bf16[64,128]{1,0:T(8,128)(2,1)S(1)}, bf16[64,128]{1,0:T(8,128)(2,1)S(1)}, u32[]{:S(2)}, u32[]{:S(2)}) %collective-permute-start.4) | collective-permute-done | bytes 16416 | tf_op jit(solution)/shard_map/ppermute | solution.py:133
  17.0 1.4 %collective-permute-done.3 = bf16[64,128]{1,0:T(8,128)(2,1)S(1)} collective-permute-done((bf16[64,128]{1,0:T(8,128)(2,1)S(1)}, bf16[64,128]{1,0:T(8,128)(2,1)S(1)}, u32[]{:S(2)}, u32[]{:S(2)}) %collective-permute-start.3) | collective-permute-done | bytes 16416 | tf_op jit(solution)/shard_map/ppermute | solution.py:133
  18.4 1.6 %collective-permute-start.6 = (bf16[64,128]{1,0:T(8,128)(2,1)S(1)}, bf16[64,128]{1,0:T(8,128)(2,1)S(1)}, u32[]{:S(2)}, u32[]{:S(2)}) collective-permute-start(bf16[64,128]{1,0:T(8,128)(2,1)S(1)} %get-tuple-element.15), channel_id=1, source_target_pairs={{0,8},{2,10},{4,12},{6,14},{8,16},{10,18},{12,20},{14,22},{16,24},... | collective-permute-start | bytes 49160 | tf_op jit(solution)/shard_map/ppermute | solution.py:111
  20.1 0.0 collective-permute-done
  20.1 1.1 %row_blocks.1 = bf16[16,128,128]{2,1,0:T(8,128)(2,1)} custom-call(bf16[128,128]{1,0:T(8,128)(2,1)S(1)} %add_convert_fusion.reduced_ref, bf16[128,2048]{1,0:T(8,128)(2,1)S(1)} %copy-done.1), custom_call_target="tpu_custom_call" | custom-call | tf_op jit(solution)/shard_map/row_blocks/pallas_call | solution.py:101
  21.2 5.1 %all-to-all-start = ((bf16[16,128,128]{2,1,0:T(8,128)(2,1)}), bf16[16,128,128]{2,1,0:T(8,128)(2,1)S(1)}, u32[]{:S(2)}, u32[]{:S(2)}) async-start(bf16[16,128,128]{2,1,0:T(8,128)(2,1)} %row_blocks.1), calls=%async_computation | async-start | bytes 1048576 | tf_op jit(solution)/shard_map/all_to_all | solution.py:185
  26.3 2.8 %collective-permute-start.7 = (bf16[64,128]{1,0:T(8,128)(2,1)S(1)}, bf16[64,128]{1,0:T(8,128)(2,1)S(1)}, u32[]{:S(2)}, u32[]{:S(2)}) collective-permute-start(bf16[64,128]{1,0:T(8,128)(2,1)S(1)} %get-tuple-element.15), channel_id=1, source_target_pairs={{0,16},{2,18},{4,20},{6,22},{8,24},{10,26},{12,28},{14,30},{16,0},... | collective-permute-start | bytes 49160 | tf_op jit(solution)/shard_map/ppermute | solution.py:111
  29.1 1.5 %collective-permute-start.8 = (bf16[64,128]{1,0:T(8,128)(2,1)S(1)}, bf16[64,128]{1,0:T(8,128)(2,1)S(1)}, u32[]{:S(2)}, u32[]{:S(2)}) collective-permute-start(bf16[64,128]{1,0:T(8,128)(2,1)S(1)} %get-tuple-element.15), channel_id=1, source_target_pairs={{0,24},{2,26},{4,28},{6,30},{8,0},{10,2},{12,4},{14,6},{16,8},{18,... | collective-permute-start | bytes 49160 | tf_op jit(solution)/shard_map/ppermute | solution.py:111
  30.6 0.0 collective-permute-done.6
  30.6 8.8 %collective-permute-done.7 = bf16[64,128]{1,0:T(8,128)(2,1)S(1)} collective-permute-done((bf16[64,128]{1,0:T(8,128)(2,1)S(1)}, bf16[64,128]{1,0:T(8,128)(2,1)S(1)}, u32[]{:S(2)}, u32[]{:S(2)}) %collective-permute-start.7) | collective-permute-done | bytes 16416 | tf_op jit(solution)/shard_map/ppermute | solution.py:111
  39.4 0.0 collective-permute-done.8
  39.4 0.0 copy-start.4
  39.5 0.0 copy-start.5
  39.5 1.5 %collective-permute-start.9 = (bf16[64,128]{1,0:T(8,128)(2,1)S(1)}, bf16[64,128]{1,0:T(8,128)(2,1)S(1)}, u32[]{:S(2)}, u32[]{:S(2)}) collective-permute-start(bf16[64,128]{1,0:T(8,128)(2,1)S(1)} %reduce_sum.32), channel_id=1, source_target_pairs={{0,2},{2,4},{4,6},{6,0},{8,10},{10,12},{12,14},{14,8},{16,18},{18,... | collective-permute-start | bytes 49160 | tf_op jit(solution)/shard_map/ppermute | solution.py:111
  41.0 1.4 %collective-permute-start.10 = (bf16[64,128]{1,0:T(8,128)(2,1)S(1)}, bf16[64,128]{1,0:T(8,128)(2,1)S(1)}, u32[]{:S(2)}, u32[]{:S(2)}) collective-permute-start(bf16[64,128]{1,0:T(8,128)(2,1)S(1)} %reduce_sum.32), channel_id=1, source_target_pairs={{0,4},{2,6},{4,0},{6,2},{8,12},{10,14},{12,8},{14,10},{16,20},{18,... | collective-permute-start | bytes 49160 | tf_op jit(solution)/shard_map/ppermute | solution.py:111
  42.4 1.5 %collective-permute-start.11 = (bf16[64,128]{1,0:T(8,128)(2,1)S(1)}, bf16[64,128]{1,0:T(8,128)(2,1)S(1)}, u32[]{:S(2)}, u32[]{:S(2)}) collective-permute-start(bf16[64,128]{1,0:T(8,128)(2,1)S(1)} %reduce_sum.32), channel_id=1, source_target_pairs={{0,6},{2,0},{4,2},{6,4},{8,14},{10,8},{12,10},{14,12},{16,22},{18,... | collective-permute-start | bytes 49160 | tf_op jit(solution)/shard_map/ppermute | solution.py:111
  43.9 0.3 collective-permute-done.9
  44.2 0.6 %collective-permute-done.10 = bf16[64,128]{1,0:T(8,128)(2,1)S(1)} collective-permute-done((bf16[64,128]{1,0:T(8,128)(2,1)S(1)}, bf16[64,128]{1,0:T(8,128)(2,1)S(1)}, u32[]{:S(2)}, u32[]{:S(2)}) %collective-permute-start.10) | collective-permute-done | bytes 16416 | tf_op jit(solution)/shard_map/ppermute | solution.py:111
  44.8 1.4 %collective-permute-done.11 = bf16[64,128]{1,0:T(8,128)(2,1)S(1)} collective-permute-done((bf16[64,128]{1,0:T(8,128)(2,1)S(1)}, bf16[64,128]{1,0:T(8,128)(2,1)S(1)}, u32[]{:S(2)}, u32[]{:S(2)}) %collective-permute-start.11) | collective-permute-done | bytes 16416 | tf_op jit(solution)/shard_map/ppermute | solution.py:111
  46.2 0.0 copy-start.7
  46.2 0.8 %updated_taps.1 = (f32[31,1024]{1,0:T(8,128)}, f32[31,1024]{1,0:T(8,128)}, f32[31,1024]{1,0:T(8,128)}) custom-call(bf16[256,128]{1,0:T(8,128)(2,1)S(1)} %bitcast.44, f32[31,1024]{1,0:T(8,128)S(1)} %copy-done.4, f32[31,1024]{1,0:T(8,128)S(1)} %copy-done.5, f32[31,1024]{1,0:T(8,128)S(1)} %copy-done.6), custom_call_target="tpu_custom_call" | custom-call | tf_op jit(solution)/shard_map/updated_taps/pallas_call | solution.py:155
  47.0 0.0 all-to-all-done
  47.0 0.1 convert_reduce_fusion
  47.1 0.0 copy-start.8
  47.1 0.0 copy-start.9
  47.1 0.1 copy.19
  47.2 0.7 %copy-done.8 = f32[128,128]{1,0:T(8,128)S(1)} copy-done((f32[128,128]{1,0:T(8,128)S(1)}, f32[128,128]{1,0:T(8,128)}, u32[]{:S(2)}) %copy-start.8) | copy-done | bytes 65560
  47.9 0.0 copy-done.9
  47.9 0.7 %multiply_convert_fusion = (bf16[128,128]{1,0:T(8,128)(2,1)S(1)}, f32[128,128]{1,0:T(8,128)}, f32[128,128]{1,0:T(8,128)}) fusion(f32[128,128]{0,1:T(8,128)S(1)} %copy.19, f32[128,128]{1,0:T(8,128)S(1)} %copy-done.8, f32[128,128]{1,0:T(8,128)S(1)} %copy-done.9), kind=kLoop, calls=%fused_computation.10 | loop fusion | flops 147456 | bytes 360448 | tf_op jit(solution)/shard_map/convert_element_type | solution.py:195
  48.6 1.9 %all_gather.3 = bf16[128,256]{1,0:T(8,128)(2,1)S(1)} all-gather(bf16[128,128]{1,0:T(8,128)(2,1)S(1)} %get-tuple-element.18), channel_id=1, replica_groups=mesh['fs'=16,'tp'=2] {'tp'}, dimensions={1}, use_global_device_ids=true | all-gather | bytes 98304 | tf_op jit(solution)/shard_map/all_gather | solution.py:195
  50.5 0.0 collective-permute-done.1
  50.5 1.3 %fusion = f32[128]{0:T(128)S(1)} fusion(bf16[128,256]{1,0:T(8,128)(2,1)S(1)} %all_gather.3, f32[256,256]{1,0:T(8,128)S(1)} %fusion.12, f32[256,256]{1,0:T(8,128)} %collective-permute-done.1), kind=kOutput, calls=%fused_computation.2 | convolution fusion | flops 100827008 | bytes 590336 | tf_op jit(solution)/shard_map/dot_general | solution.py:200
  51.8 2.0 %fusion.8 = (bf16[128,2048]{1,0:T(8,128)(2,1)}, f32[128,2048]{1,0:T(8,128)}, f32[128,2048]{1,0:T(8,128)}) fusion(f32[128,2048]{1,0:T(8,128)S(1)} %copy-done.7, f32[128]{0:T(128)S(1)} %add_rsqrt_fusion, bf16[128,256]{1,0:T(8,128)(2,1)S(1)} %all_gather.3, bf16[2048,256]{1,0:T(8,128)(2,1)S(1)} %copy-done), kind=kOutput, calls=%fused_computation.29 | convolution fusion | flops 135266304 | bytes 4784640 | tf_op jit(solution)/shard_map/dot_general | solution.py:196
  (25 shorter events, 0.2 us)
Async XLA Ops:
  0.6 5.8 %copy-start = (bf16[2048,256]{1,0:T(8,128)(2,1)S(1)}, bf16[2048,256]{1,0:T(8,128)(2,1)}, u32[]{:S(2)}) copy-start(bf16[2048,256]{1,0:T(8,128)(2,1)} %param.15) | copy-start | bytes 3145732
  1.6 6.8 %collective-permute-start.2 = (bf16[32,1024]{1,0:T(8,128)(2,1)S(1)}, bf16[32,1024]{1,0:T(8,128)(2,1)S(1)}, u32[]{:S(2)}, u32[]{:S(2)}) collective-permute-start(bf16[32,1024]{1,0:T(8,128)(2,1)S(1)} %slice.3), channel_id=1, source_target_pairs={{0,2},{2,4},{4,6},{6,8},{8,10},{10,12},{12,14},{14,16},{16,18},{18... | collective-permute-start | bytes 196616 | tf_op jit(solution)/shard_map/ppermute | solution.py:15
  6.5 1.9 %copy-start.2 = (bf16[128,1024]{1,0:T(8,128)(2,1)S(1)}, bf16[128,1024]{1,0:T(8,128)(2,1)}, u32[]{:S(2)}) copy-start(bf16[128,1024]{1,0:T(8,128)(2,1)} %tokens_ref.1) | copy-start | bytes 786436
  6.5 1.9 %copy-start.3 = (bf16[128,1024]{1,0:T(8,128)(2,1)S(1)}, bf16[128,1024]{1,0:T(8,128)(2,1)}, u32[]{:S(2)}) copy-start(bf16[128,1024]{1,0:T(8,128)(2,1)} %cot_ref.3) | copy-start | bytes 786436
  7.9 12.1 %collective-permute-start = (bf16[128,128]{1,0:T(8,128)(2,1)S(1)}, bf16[128,128]{1,0:T(8,128)(2,1)S(1)}, u32[]{:S(2)}, u32[]{:S(2)}) collective-permute-start(bf16[128,128]{1,0:T(8,128)(2,1)S(1)} %dynamic-slice_convert_fusion), channel_id=1, source_target_pairs={{0,1},{1,0},{2,3},{3,2},{4,5},{5,4},{6,7},{7,6},{8,9},{9,8},{10,11... | collective-permute-start | bytes 98312 | tf_op jit(solution)/shard_map/ppermute | solution.py:27
  9.9 6.1 %collective-permute-start.5 = (bf16[64,128]{1,0:T(8,128)(2,1)S(1)}, bf16[64,128]{1,0:T(8,128)(2,1)S(1)}, u32[]{:S(2)}, u32[]{:S(2)}) collective-permute-start(bf16[64,128]{1,0:T(8,128)(2,1)S(1)} %get-tuple-element.22), channel_id=1, source_target_pairs={{0,6},{2,0},{4,2},{6,4},{8,14},{10,8},{12,10},{14,12},{16,22},{18,... | collective-permute-start | bytes 49160 | tf_op jit(solution)/shard_map/ppermute | solution.py:133
  13.2 3.7 %collective-permute-start.4 = (bf16[64,128]{1,0:T(8,128)(2,1)S(1)}, bf16[64,128]{1,0:T(8,128)(2,1)S(1)}, u32[]{:S(2)}, u32[]{:S(2)}) collective-permute-start(bf16[64,128]{1,0:T(8,128)(2,1)S(1)} %get-tuple-element.23), channel_id=1, source_target_pairs={{0,4},{2,6},{4,0},{6,2},{8,12},{10,14},{12,8},{14,10},{16,20},{18,... | collective-permute-start | bytes 49160 | tf_op jit(solution)/shard_map/ppermute | solution.py:133
  13.8 4.6 %collective-permute-start.3 = (bf16[64,128]{1,0:T(8,128)(2,1)S(1)}, bf16[64,128]{1,0:T(8,128)(2,1)S(1)}, u32[]{:S(2)}, u32[]{:S(2)}) collective-permute-start(bf16[64,128]{1,0:T(8,128)(2,1)S(1)} %get-tuple-element.21), channel_id=1, source_target_pairs={{0,2},{2,4},{4,6},{6,0},{8,10},{10,12},{12,14},{14,8},{16,18},{18,... | collective-permute-start | bytes 49160 | tf_op jit(solution)/shard_map/ppermute | solution.py:133
  15.2 4.8 %copy-start.1 = (bf16[128,2048]{1,0:T(8,128)(2,1)S(1)}, bf16[128,2048]{1,0:T(8,128)(2,1)}, u32[]{:S(2)}) copy-start(bf16[128,2048]{1,0:T(8,128)(2,1)} %cot_ref.2) | copy-start | bytes 1572868
  15.7 34.8 %collective-permute-start.1 = (f32[256,256]{1,0:T(8,128)S(1)}, f32[256,256]{1,0:T(8,128)}, u32[]{:S(2)}, u32[]{:S(2)}) collective-permute-start(f32[256,256]{1,0:T(8,128)S(1)} %fusion.12), channel_id=1, source_target_pairs={{0,1},{1,0},{2,3},{3,2},{4,5},{5,4},{6,7},{7,6},{8,9},{9,8},{10,11... | collective-permute-start | bytes 786440 | tf_op jit(solution)/shard_map/ppermute | solution.py:36
  18.4 12.1 %collective-permute-start.6 = (bf16[64,128]{1,0:T(8,128)(2,1)S(1)}, bf16[64,128]{1,0:T(8,128)(2,1)S(1)}, u32[]{:S(2)}, u32[]{:S(2)}) collective-permute-start(bf16[64,128]{1,0:T(8,128)(2,1)S(1)} %get-tuple-element.15), channel_id=1, source_target_pairs={{0,8},{2,10},{4,12},{6,14},{8,16},{10,18},{12,20},{14,22},{16,24},... | collective-permute-start | bytes 49160 | tf_op jit(solution)/shard_map/ppermute | solution.py:111
  21.2 24.9 %copy-start.6 = (f32[31,1024]{1,0:T(8,128)S(1)}, f32[31,1024]{1,0:T(8,128)}, u32[]{:S(2)}) copy-start(f32[31,1024]{1,0:T(8,128)} %second_ref.1) | copy-start | bytes 380932
  21.2 25.8 %all-to-all-start = ((bf16[16,128,128]{2,1,0:T(8,128)(2,1)}), bf16[16,128,128]{2,1,0:T(8,128)(2,1)S(1)}, u32[]{:S(2)}, u32[]{:S(2)}) async-start(bf16[16,128,128]{2,1,0:T(8,128)(2,1)} %row_blocks.1), calls=%async_computation | async-start | bytes 1048576 | tf_op jit(solution)/shard_map/all_to_all | solution.py:185
  26.3 13.1 %collective-permute-start.7 = (bf16[64,128]{1,0:T(8,128)(2,1)S(1)}, bf16[64,128]{1,0:T(8,128)(2,1)S(1)}, u32[]{:S(2)}, u32[]{:S(2)}) collective-permute-start(bf16[64,128]{1,0:T(8,128)(2,1)S(1)} %get-tuple-element.15), channel_id=1, source_target_pairs={{0,16},{2,18},{4,20},{6,22},{8,24},{10,26},{12,28},{14,30},{16,0},... | collective-permute-start | bytes 49160 | tf_op jit(solution)/shard_map/ppermute | solution.py:111
  29.1 10.3 %collective-permute-start.8 = (bf16[64,128]{1,0:T(8,128)(2,1)S(1)}, bf16[64,128]{1,0:T(8,128)(2,1)S(1)}, u32[]{:S(2)}, u32[]{:S(2)}) collective-permute-start(bf16[64,128]{1,0:T(8,128)(2,1)S(1)} %get-tuple-element.15), channel_id=1, source_target_pairs={{0,24},{2,26},{4,28},{6,30},{8,0},{10,2},{12,4},{14,6},{16,8},{18,... | collective-permute-start | bytes 49160 | tf_op jit(solution)/shard_map/ppermute | solution.py:111
  39.4 6.7 %copy-start.4 = (f32[31,1024]{1,0:T(8,128)S(1)}, f32[31,1024]{1,0:T(8,128)}, u32[]{:S(2)}) copy-start(f32[31,1024]{1,0:T(8,128)} %kernel_ref.1) | copy-start | bytes 380932
  39.5 6.7 %copy-start.5 = (f32[31,1024]{1,0:T(8,128)S(1)}, f32[31,1024]{1,0:T(8,128)}, u32[]{:S(2)}) copy-start(f32[31,1024]{1,0:T(8,128)} %first_ref.1) | copy-start | bytes 380932
  39.5 4.7 %collective-permute-start.9 = (bf16[64,128]{1,0:T(8,128)(2,1)S(1)}, bf16[64,128]{1,0:T(8,128)(2,1)S(1)}, u32[]{:S(2)}, u32[]{:S(2)}) collective-permute-start(bf16[64,128]{1,0:T(8,128)(2,1)S(1)} %reduce_sum.32), channel_id=1, source_target_pairs={{0,2},{2,4},{4,6},{6,0},{8,10},{10,12},{12,14},{14,8},{16,18},{18,... | collective-permute-start | bytes 49160 | tf_op jit(solution)/shard_map/ppermute | solution.py:111
  41.0 3.7 %collective-permute-start.10 = (bf16[64,128]{1,0:T(8,128)(2,1)S(1)}, bf16[64,128]{1,0:T(8,128)(2,1)S(1)}, u32[]{:S(2)}, u32[]{:S(2)}) collective-permute-start(bf16[64,128]{1,0:T(8,128)(2,1)S(1)} %reduce_sum.32), channel_id=1, source_target_pairs={{0,4},{2,6},{4,0},{6,2},{8,12},{10,14},{12,8},{14,10},{16,20},{18,... | collective-permute-start | bytes 49160 | tf_op jit(solution)/shard_map/ppermute | solution.py:111
  42.4 3.7 %collective-permute-start.11 = (bf16[64,128]{1,0:T(8,128)(2,1)S(1)}, bf16[64,128]{1,0:T(8,128)(2,1)S(1)}, u32[]{:S(2)}, u32[]{:S(2)}) collective-permute-start(bf16[64,128]{1,0:T(8,128)(2,1)S(1)} %reduce_sum.32), channel_id=1, source_target_pairs={{0,6},{2,0},{4,2},{6,4},{8,14},{10,8},{12,10},{14,12},{16,22},{18,... | collective-permute-start | bytes 49160 | tf_op jit(solution)/shard_map/ppermute | solution.py:111
  46.2 5.6 %copy-start.7 = (f32[128,2048]{1,0:T(8,128)S(1)}, f32[128,2048]{1,0:T(8,128)}, u32[]{:S(2)}) copy-start(f32[128,2048]{1,0:T(8,128)} %param.16) | copy-start | bytes 3145732
  47.1 0.8 %copy-start.8 = (f32[128,128]{1,0:T(8,128)S(1)}, f32[128,128]{1,0:T(8,128)}, u32[]{:S(2)}) copy-start(f32[128,128]{1,0:T(8,128)} %param.18) | copy-start | bytes 196612
  47.1 0.9 %copy-start.9 = (f32[128,128]{1,0:T(8,128)S(1)}, f32[128,128]{1,0:T(8,128)}, u32[]{:S(2)}) copy-start(f32[128,128]{1,0:T(8,128)} %param.17) | copy-start | bytes 196612
